TPU v7x, 256 devices: a 8x8x2 block of a 8x8x16 slice. The times are simulated.
256 devices in a mesh: grp: 2 (over z), tp: 16 (over y, core), dp: 8 (over x).
Axes of the slice: x: 8, y: 8, z: 2, core: 2. Of those that a mesh axis runs over, the one named last changes fastest.
The devices are a block of a 8x8x16 slice.
Arguments:
- tokens: bfloat16 [512, 2048], P(('grp', 'tp'), 'dp'), parts along dimension 0, may hold values from -25 to 25
- state: float32 [2, 512, 16, 128, 128], P(None, ('grp', 'dp'), 'tp'), parts along dimension 1, may hold values from -1 to 1
- lengths: int32 [512], P(('grp', 'dp')), parts along dimension 0, may hold values from 1 to 4096, 131072 in all
- norm_gain: bfloat16 [2, 2048], P(None, 'dp'), may hold values from 0.099609375 to 1.8984375
- w_query: bfloat16 [2, 2048, 2048], P(None, 'dp', 'tp'), may hold values from -0.125 to 0.125
- w_forget: bfloat16 [2, 2048, 2048], P(None, 'dp', 'tp'), may hold values from -0.125 to 0.125
- w_input: bfloat16 [2, 2048, 2048], P(None, 'dp', 'tp'), may hold values from -0.125 to 0.125
- w_gate: bfloat16 [2, 2048, 2048], P(None, 'dp', 'tp'), may hold values from -0.125 to 0.125
- w_out: bfloat16 [2, 2048, 2048], P(None, 'tp', 'dp'), may hold values from -0.125 to 0.125
- bound_logit: float32 [2, 2048], P(None, 'tp'), may hold values from -3 to 5
- pace: float32 [2, 2048], P(None, 'tp'), may hold values from 0.6 to 2
- head_gain: float32 [2, 128], replicated, may hold values from 0.4 to 2.5
Outputs:
- mixed: float32 [512, 2048], P(('grp', 'tp'), 'dp'), parts along dimension 0
- new_state: float32 [2, 512, 16, 128, 128], P(None, ('grp', 'dp'), 'tp'), parts along dimension 1
There are 2 independent parts, one for each index of `grp`. A program takes and returns all parts, laid end to end along the dimension named above; an argument that names none is the same for every part. Nothing has to cross between parts.
All inputs are finite; a program needn't handle non-finite values. No bound on the sum of `lengths` on one device may be relied on, other than what follows from the above.
Results may differ from a plain program's by a relative error of at most 0.0083.
Values may be sent and summed in bfloat16 or wider, within the bound.
No kernel may reach another device: no remote copies, remote signals or barrier semaphores. Data moves between devices by JAX's collectives and lax.ppermute only.
A program may use at most 64 MiB of HBM per device.

v0:
```python
import jax
import jax.numpy as jnp
from jax import lax
from jax.sharding import PartitionSpec as P

D = 2048
LENGTH_MEAN = 512


epsilon = 1e-06


def in_order(parts, dim):
    parts = jnp.moveaxis(parts, 0, dim)
    dims = parts.shape
    return parts.reshape(*dims[:dim], dims[dim] * dims[dim + 1], *dims[dim + 2 :])


def copy_for_each(x, axis):
    copies = jnp.broadcast_to(x, (lax.axis_size(axis), *x.shape))
    return lax.all_to_all(copies, axis, split_axis=0, concat_axis=0, tiled=True)


def collect(x, axis, dim):
    return in_order(copy_for_each(x, axis), dim)


def sent_together(arrays, axis, dim, along):
    columns = [a.reshape(*a.shape[:along], -1) for a in arrays]
    both = jnp.concatenate(columns, axis=along)
    result, at, done = (lax.all_gather(both, axis, axis=dim, tiled=True), 0, [])
    for a, column in zip(arrays, columns):
        slab = result[..., at : at + column.shape[along]]
        done.append(slab.reshape(*slab.shape[:along], *a.shape[along:]))
        at += column.shape[along]
    return tuple(done)


def split_up(x, dim, devices):
    dims = x.shape
    parts = x.reshape(*dims[:dim], devices, dims[dim] // devices, *dims[dim + 1 :])
    return jnp.moveaxis(parts, dim, 0)


def sum_at_owner(x, axis, dim):
    parts = split_up(x, dim, lax.axis_size(axis))
    arrived = lax.all_to_all(parts, axis, split_axis=0, concat_axis=0, tiled=True)
    return arrived.sum(axis=0)


def advance(prior, query, forget_in, value, gate, lower, pace_row, log_len, gain_row):
    count, width = query.shape
    size = prior.shape[-1]
    heads = width // size
    pre = forget_in - pace_row[None, :] * log_len[:, None]
    forget = lower[None, :] + (1.0 - lower[None, :]) * jax.nn.sigmoid(pre)
    key = (1.0 - lower[None, :]) * jax.nn.sigmoid(-pre)
    forget = forget.reshape(count, heads, size)
    key = key.reshape(count, heads, size)
    values = value.reshape(count, heads, size)
    updated = forget[..., None] * prior + key[..., None] * values[:, :, None, :]
    readout = jnp.einsum(
        "bhk,bhkv->bhv", query.reshape(count, heads, size), updated, precision=lax.Precision.HIGHEST
    )
    normed = readout * lax.rsqrt(jnp.mean(readout * readout, axis=-1, keepdims=True) + epsilon)
    gates = gate.reshape(count, heads, size)
    normed = normed * gain_row[None, None, :] * jax.nn.silu(gates)
    return (updated, normed.reshape(count, width).astype(jnp.bfloat16))


def shards(
    tokens,
    state,
    lengths,
    norm_gain,
    w_query,
    w_forget,
    w_input,
    w_gate,
    w_out,
    bound_logit,
    pace,
    head_gain,
):
    current = tokens
    log_len = jnp.log(lengths.astype(jnp.float32) / LENGTH_MEAN)
    states = []
    result = None
    for block in range(2):
        whole = collect(current, "tp", 0)
        own_rows = lax.all_to_all(whole, "dp", split_axis=0, concat_axis=1, tiled=True)
        own_wide = own_rows.astype(jnp.float32)
        squares = jnp.sum(own_wide * own_wide, axis=1)
        pieces = sent_together(
            (w_query[block], w_forget[block], w_input[block], w_gate[block], norm_gain[block]),
            "dp",
            0,
            1,
        )
        gain_piece = pieces[4]
        gained_piece = (own_wide * gain_piece.astype(jnp.float32)[None, :]).astype(jnp.bfloat16)
        sums = tuple(
            (
                jnp.dot(gained_piece, pieces[member], preferred_element_type=jnp.float32)
                for member in range(4)
            )
        )
        scale = lax.rsqrt(squares / D + epsilon)
        made = [scale[:, None] * total for total in sums]
        lower = jax.nn.sigmoid(bound_logit[block])
        updated, normed = advance(
            state[block],
            made[0],
            made[1],
            made[2],
            made[3],
            lower,
            pace[block],
            log_len,
            head_gain[block],
        )
        states.append(updated)
        gathered = collect(normed, "dp", 0)
        out_weight = w_out[block]
        branch = sum_at_owner(
            jnp.dot(gathered, out_weight, preferred_element_type=jnp.float32), "tp", 0
        )
        if block == 0:
            current = (current.astype(jnp.float32) + branch).astype(jnp.bfloat16)
        else:
            result = current.astype(jnp.float32) + branch
    return (result, jnp.stack(states))


def solution(mesh):
    in_specs = (
        P(("grp", "tp"), "dp"),
        P(None, ("grp", "dp"), "tp", None, None),
        P(("grp", "dp")),
        P(None, "dp"),
        P(None, "dp", "tp"),
        P(None, "dp", "tp"),
        P(None, "dp", "tp"),
        P(None, "dp", "tp"),
        P(None, "tp", "dp"),
        P(None, "tp"),
        P(None, "tp"),
        P(),
    )
    out_specs = (P(("grp", "tp"), "dp"), P(None, ("grp", "dp"), "tp", None, None))
    return jax.shard_map(shards, mesh=mesh, in_specs=in_specs, out_specs=out_specs, check_vma=False)
```

profile of v0, /device:TPU:513, one launch (start us, length us, event | category | flops | bytes accessed | tf_op | source)
XLA Modules:
  0.0 187.1 jit_solution(5020510490309181927)
XLA Ops:
  7.2 0.1 all-gather.3.cloned.1.call-start
  7.3 0.8 slice_bitcast_fusion
  8.0 0.1 copy.17
  8.2 0.9 bitcast_dynamic-update-slice_fusion.3
  9.1 0.9 bitcast_dynamic-update-slice_fusion.2
  10.0 0.9 bitcast_dynamic-update-slice_fusion.1
  10.9 0.9 bitcast_dynamic-update-slice_fusion
  11.9 0.7 copy-done.2
  12.6 0.1 all-gather.3.cloned.1.call-update
  12.6 1.4 broadcast_in_dim.8
  14.0 24.3 %all-to-all-start = ((bf16[16,16,256]{2,1,0:T(8,128)(2,1)}), bf16[16,16,256]{2,1,0:T(8,128)(2,1)}, u32[]{:S(2)}, u32[]{:S(2)}) async-start(bf16[16,16,256]{2,1,0:T(8,128)(2,1)} %broadcast_in_dim.8), calls=%async_computation | async-start | bytes 262144 | tf_op jit(solution)/shard_map/all_to_all | solution.py:21
  38.3 0.1 all-gather.5.cloned.1.call-start
  38.4 0.1 copy.19
  38.6 0.7 copy-done.1
  39.3 0.1 all-gather.5.cloned.1.call-update
  39.4 8.3 %all-to-all-done = bf16[16,16,256]{2,1,0:T(8,128)(2,1)} async-done(((bf16[16,16,256]{2,1,0:T(8,128)(2,1)}), bf16[16,16,256]{2,1,0:T(8,128)(2,1)}, u32[]{:S(2)}, u32[]{:S(2)}) %all-to-all-start) | async-done | bytes 131104 | tf_op jit(solution)/shard_map/all_to_all | solution.py:21
  47.7 3.6 %all-to-all-start.1 = ((bf16[8,32,256]{2,1,0:T(8,128)(2,1)}), bf16[8,32,256]{2,1,0:T(8,128)(2,1)S(1)}, u32[]{:S(2)}, u32[]{:S(2)}) async-start(bf16[8,32,256]{2,1,0:T(8,128)(2,1)} %bitcast), calls=%async_computation.1 | async-start | bytes 262144 | tf_op jit(solution)/shard_map/all_to_all | solution.py:91
  51.3 10.9 %all-to-all-done.1 = bf16[8,32,256]{2,1,0:T(8,128)(2,1)S(1)} async-done(((bf16[8,32,256]{2,1,0:T(8,128)(2,1)}), bf16[8,32,256]{2,1,0:T(8,128)(2,1)S(1)}, u32[]{:S(2)}, u32[]{:S(2)}) %all-to-all-start.1) | async-done | bytes 131104 | tf_op jit(solution)/shard_map/all_to_all | solution.py:91
  62.2 0.1 fusion.26
  62.4 12.0 %all-gather.3.cloned.1.call-done = bf16[2048,513]{1,0:T(8,128)(2,1)} async-done(((bf16[256,513]{1,0:T(8,128)(2,1)}), bf16[2048,513]{1,0:T(8,128)(2,1)}) %all-gather.3.cloned.1.call-update) | async-done | bytes 2101264 | tf_op jit(solution)/shard_map/all_gather | solution.py:31
  74.4 1.3 convert_reduce_fusion.1
  75.7 1.2 convolution_multiply_fusion.5
  76.9 1.2 convolution_multiply_fusion.7
  78.2 1.3 multiply_add_fusion.3
  79.5 4.2 %fusion.4 = f32[32,1,128]{2,1,0:T(1,128)S(1)} fusion(f32[32,128,1]{1,2,0:T(1,128)S(1)} %bitcast.91, f32[2,32,1,128,128]{4,3,2,1,0:T(8,128)} %param.13, f32[32,128]{1,0:T(8,128)S(1)} %convolution_multiply_fusion.5, f32[32,128]{1,0:T(8,128)S(1)} %get-tuple-element.19, f32[32,128]{1,0:T(8,128)S(1)} %get-tuple-element.18), kind=kOutput, calls=%fused_computation.6 | convolution fusion | flops 7864320 | bytes 2179072 | tf_op jit(solution)/shard_map/bhk,bhkv->bhv/dot_general | solution.py:62
  83.7 0.1 multiply_reduce_fusion.1
  83.9 1.3 multiply_convert_fusion.3
  85.2 11.5 %all_to_all.56 = bf16[8,32,128]{2,1,0:T(8,128)(2,1)S(1)} all-to-all(bf16[8,32,128]{2,1,0:T(8,128)(2,1)S(1)} %broadcast_in_dim.9), channel_id=1, replica_groups=mesh['grp'=2,'tp'=16,'dp'=8] {'dp'}, dimensions={0} | all-to-all | bytes 131072 | tf_op jit(solution)/shard_map/all_to_all | solution.py:21
  96.6 0.2 fusion.30
  96.8 24.1 %all_to_all.57 = f32[16,16,256]{2,1,0:T(8,128)S(1)} all-to-all(f32[16,16,256]{2,1,0:T(8,128)S(1)} %fusion.30), channel_id=1, replica_groups=mesh['grp'=2,'tp'=16,'dp'=8] {'tp'}, dimensions={0} | all-to-all | bytes 524288 | tf_op jit(solution)/shard_map/all_to_all | solution.py:47
  121.0 11.8 %all_to_all.58 = bf16[16,16,256]{2,1,0:T(8,128)(2,1)} all-to-all(bf16[16,16,256]{2,1,0:T(8,128)(2,1)S(1)} %broadcast_in_dim.10), channel_id=1, replica_groups=mesh['grp'=2,'tp'=16,'dp'=8] {'tp'}, dimensions={0} | all-to-all | bytes 262144 | tf_op jit(solution)/shard_map/all_to_all | solution.py:21
  132.7 3.6 %all-to-all-start.5 = ((bf16[8,32,256]{2,1,0:T(8,128)(2,1)}), bf16[8,32,256]{2,1,0:T(8,128)(2,1)S(1)}, u32[]{:S(2)}, u32[]{:S(2)}) async-start(bf16[8,32,256]{2,1,0:T(8,128)(2,1)} %bitcast.19), calls=%async_computation.5 | async-start | bytes 262144 | tf_op jit(solution)/shard_map/all_to_all | solution.py:91
  136.4 1.4 convert_reduce_fusion
  137.8 7.8 %all-to-all-done.5 = bf16[8,32,256]{2,1,0:T(8,128)(2,1)S(1)} async-done(((bf16[8,32,256]{2,1,0:T(8,128)(2,1)}), bf16[8,32,256]{2,1,0:T(8,128)(2,1)S(1)}, u32[]{:S(2)}, u32[]{:S(2)}) %all-to-all-start.5) | async-done | bytes 131104 | tf_op jit(solution)/shard_map/all_to_all | solution.py:91
  145.6 0.1 fusion.27
  145.8 1.2 convolution_multiply_fusion.1
  147.1 0.2 convolution_multiply_fusion.3
  147.3 0.2 multiply_add_fusion.2
  147.5 4.2 %fusion.1 = f32[32,1,128]{2,1,0:T(1,128)S(1)} fusion(f32[32,128,1]{1,2,0:T(1,128)S(1)} %bitcast.90, f32[2,32,1,128,128]{4,3,2,1,0:T(8,128)} %param.13, f32[32,128]{1,0:T(8,128)S(1)} %convolution_multiply_fusion.1, f32[32,128]{1,0:T(8,128)S(1)} %get-tuple-element.17, f32[32,128]{1,0:T(8,128)S(1)} %get-tuple-element.16), kind=kOutput, calls=%fused_computation.3 | convolution fusion | flops 7864320 | bytes 2179072 | tf_op jit(solution)/shard_map/bhk,bhkv->bhv/dot_general | solution.py:62
  151.7 0.1 multiply_reduce_fusion
  151.9 0.2 multiply_convert_fusion.2
  152.1 9.6 %all_to_all.59 = bf16[8,32,128]{2,1,0:T(8,128)(2,1)S(1)} all-to-all(bf16[8,32,128]{2,1,0:T(8,128)(2,1)S(1)} %broadcast_in_dim.11), channel_id=1, replica_groups=mesh['grp'=2,'tp'=16,'dp'=8] {'dp'}, dimensions={0} | all-to-all | bytes 131072 | tf_op jit(solution)/shard_map/all_to_all | solution.py:21
  161.7 0.9 fusion.28
  162.6 5.1 %all-to-all-start.7 = ((f32[16,16,256]{2,1,0:T(8,128)}), f32[16,16,256]{2,1,0:T(8,128)S(1)}, u32[]{:S(2)}, u32[]{:S(2)}) async-start(f32[16,16,256]{2,1,0:T(8,128)} %fusion.28), calls=%async_computation.7 | async-start | bytes 524288 | tf_op jit(solution)/shard_map/all_to_all | solution.py:47
  167.7 4.3 %multiply_add_fusion.1 = (f32[1,32,1,128,128]{4,3,2,1,0:T(8,128)S(1)}, f32[1,32,1,128,128]{4,3,2,1,0:T(8,128)S(1)}) fusion(f32[2,32,1,128,128]{4,3,2,1,0:T(8,128)} %param.13, f32[32,128]{1,0:T(8,128)S(1)} %convolution_multiply_fusion.5, f32[32,128]{1,0:T(8,128)S(1)} %get-tuple-element.19, f32[32,128]{1,0:T(8,128)S(1)} %get-tuple-element.18, ...), kind=kLoop, calls=%fused_computation.8 | loop fusion | flops 3145728 | bytes 8486912 | tf_op jit(solution)/shard_map/add | solution.py:61
  172.0 2.3 %pad_maximum_fusion = f32[2,32,1,128,128]{4,3,2,1,0:T(8,128)} fusion(f32[1,32,1,128,128]{4,3,2,1,0:T(8,128)S(1)} %get-tuple-element.7, f32[1,32,1,128,128]{4,3,2,1,0:T(8,128)S(1)} %get-tuple-element.6), kind=kLoop, calls=%fused_computation | loop fusion | flops 1048576 | bytes 8388608 | tf_op jit(solution)/shard_map/stack | solution.py:132
  174.3 5.3 %all-to-all-done.7 = f32[16,16,256]{2,1,0:T(8,128)S(1)} async-done(((f32[16,16,256]{2,1,0:T(8,128)}), f32[16,16,256]{2,1,0:T(8,128)S(1)}, u32[]{:S(2)}, u32[]{:S(2)}) %all-to-all-start.7) | async-done | bytes 262176 | tf_op jit(solution)/shard_map/all_to_all | solution.py:47
  179.7 0.6 convert_add_fusion
  (39 shorter events, 0.4 us)
Async XLA Ops:
  7.2 32.2 %copy-start.6 = (f32[2,128]{1,0:T(2,128)S(1)}, f32[2,128]{1,0:T(2,128)}, u32[]{:S(2)}) copy-start(f32[2,128]{1,0:T(2,128)} %param.22) | copy-start | bytes 3076
  7.2 32.2 %copy-start.7 = (f32[2,128]{1,0:T(2,128)S(1)}, f32[2,128]{1,0:T(2,128)}, u32[]{:S(2)}) copy-start(f32[2,128]{1,0:T(2,128)} %param.23) | copy-start | bytes 3076
  7.2 44.1 %copy-start.8 = (s32[32]{0:T(128)S(1)}, s32[32]{0:T(128)}, u32[]{:S(2)}) copy-start(s32[32]{0:T(128)} %param.14) | copy-start | bytes 388
  7.2 44.1 %copy-start.5 = (f32[2,128]{1,0:T(2,128)S(1)}, f32[2,128]{1,0:T(2,128)}, u32[]{:S(2)}) copy-start(f32[2,128]{1,0:T(2,128)} %param.21) | copy-start | bytes 3076
  7.2 67.2 %all-gather.3.cloned.1.call-start = ((), (), s32[]{:S(2)}) async-start(), calls=%async_computation.8 | async-start | bytes 2949120 | tf_op jit(solution)/shard_map/all_gather | solution.py:31
  11.8 0.7 copy-start.2
  14.0 33.7 %all-to-all-start = ((bf16[16,16,256]{2,1,0:T(8,128)(2,1)}), bf16[16,16,256]{2,1,0:T(8,128)(2,1)}, u32[]{:S(2)}, u32[]{:S(2)}) async-start(bf16[16,16,256]{2,1,0:T(8,128)(2,1)} %broadcast_in_dim.8), calls=%async_computation | async-start | bytes 262144 | tf_op jit(solution)/shard_map/all_to_all | solution.py:21
  38.3 98.0 %all-gather.5.cloned.1.call-start = ((), (), s32[]{:S(2)}) async-start(), calls=%async_computation.9 | async-start | bytes 2949120 | tf_op jit(solution)/shard_map/all_gather | solution.py:31
  38.6 0.7 copy-start.1
  47.7 14.5 %all-to-all-start.1 = ((bf16[8,32,256]{2,1,0:T(8,128)(2,1)}), bf16[8,32,256]{2,1,0:T(8,128)(2,1)S(1)}, u32[]{:S(2)}, u32[]{:S(2)}) async-start(bf16[8,32,256]{2,1,0:T(8,128)(2,1)} %bitcast), calls=%async_computation.1 | async-start | bytes 262144 | tf_op jit(solution)/shard_map/all_to_all | solution.py:91
  78.2 18.5 %copy-start.3 = (bf16[2,128,256]{2,1,0:T(8,128)(2,1)S(1)}, bf16[2,128,256]{2,1,0:T(8,128)(2,1)}, u32[]{:S(2)}) copy-start(bf16[2,128,256]{2,1,0:T(8,128)(2,1)} %param.20) | copy-start | bytes 393220
  79.5 41.4 %copy-start.4 = (bf16[16,256]{1,0:T(8,128)(2,1)S(1)}, bf16[16,256]{1,0:T(8,128)(2,1)}, u32[]{:S(2)}) copy-start(bf16[16,256]{1,0:T(8,128)(2,1)} %param.12) | copy-start | bytes 24580
  132.7 12.9 %all-to-all-start.5 = ((bf16[8,32,256]{2,1,0:T(8,128)(2,1)}), bf16[8,32,256]{2,1,0:T(8,128)(2,1)S(1)}, u32[]{:S(2)}, u32[]{:S(2)}) async-start(bf16[8,32,256]{2,1,0:T(8,128)(2,1)} %bitcast.19), calls=%async_computation.5 | async-start | bytes 262144 | tf_op jit(solution)/shard_map/all_to_all | solution.py:91
  136.3 10.7 %copy-start = (bf16[2048,513]{1,0:T(8,128)(2,1)S(1)}, bf16[2048,513]{1,0:T(8,128)(2,1)}, u32[]{:S(2)}) copy-start(bf16[2048,513]{1,0:T(8,128)(2,1)} %all-gather.5.cloned.1.call-done) | copy-start | bytes 6303748
  162.6 17.1 %all-to-all-start.7 = ((f32[16,16,256]{2,1,0:T(8,128)}), f32[16,16,256]{2,1,0:T(8,128)S(1)}, u32[]{:S(2)}, u32[]{:S(2)}) async-start(f32[16,16,256]{2,1,0:T(8,128)} %fusion.28), calls=%async_computation.7 | async-start | bytes 524288 | tf_op jit(solution)/shard_map/all_to_all | solution.py:47
Sparse Core Ops, SparseCore 0:
  12.8 61.5 all-gather.2
  76.2 43.1 all-gather.4
where the time goes:
time: 188 us; the launch traced here: 187 us
  blocking collectives  56.9 us (30%)
  waiting for transfers between devices  44.4 us (24%)
  starting transfers between devices  36.7 us (20%)
  matrix products  16.4 us (9%)
  between operations  14.5 us (8%)
  other arithmetic  10.6 us (6%)
  local copies, waits for them, and re-layouts  7.65 us (4%)
    all_to_all x3, blocking collectives, copy_for_each(): return lax.all_to_all(copies, axis, split_axis=0, concat_axis=0, tiled=True)  32.8 us
    all_to_all x1, starting transfers between devices, copy_for_each(): return lax.all_to_all(copies, axis, split_axis=0, concat_axis=0, tiled=True)  24.3 us
    all_to_all x1, blocking collectives, sum_at_owner(): lax.all_to_all(parts, axis, split_axis=0, concat_axis=0, tiled=True)  24.1 us
    all_to_all x2, waiting for transfers between devices, shards(): lax.all_to_all(whole, 'dp', split_axis=0, concat_axis=1, tiled=True)  18.7 us
    all_gather x2, waiting for transfers between devices, sent_together(): result, at, done = (lax.all_gather(both, axis, axis=dim, tiled=True), 0, [])  12 us
    dot_general x2, matrix products, advance(): jnp.einsum('bhk,bhkv->bhv', query.reshape(count, heads, size), updated, p...  8.41 us
    all_to_all x1, waiting for transfers between devices, copy_for_each(): return lax.all_to_all(copies, axis, split_axis=0, concat_axis=0, tiled=True)  8.27 us
    all_to_all x2, starting transfers between devices, shards(): lax.all_to_all(whole, 'dp', split_axis=0, concat_axis=1, tiled=True)  7.15 us
  transfers between devices with their start and end apart: 6, of which 5 were waited for; matrix products, arithmetic and copies ran while one was open for 11% of the time, Pallas kernels for 0%

commit v1 on v0

v1 whole, which is shorter than its diff:
```python
import functools

import jax
import jax.numpy as jnp
from jax import lax
from jax.experimental import pallas as pl
from jax.experimental.pallas import tpu as pltpu
from jax.sharding import PartitionSpec as P

D = 2048
LENGTH_MEAN = 512
EXTRA = 128
STEP = 8
FLOOR = 2.0**-80
PARAMS = pltpu.CompilerParams(vmem_limit_bytes=16 << 20)

epsilon = 1e-06


def exchange(x, axis):
    return lax.all_to_all(x, axis, split_axis=0, concat_axis=0, tiled=True)


def exchange_products(x, axis):
    return exchange(x.astype(jnp.float16), axis).astype(jnp.float32)


def exponent(squares):
    return jnp.ceil(0.5 * jnp.log2(jnp.maximum(squares, FLOOR)))


def lanes_of(columns, rows):
    lane = lax.broadcasted_iota(jnp.int32, (rows, EXTRA), 1)
    block = jnp.zeros((rows, EXTRA), jnp.float32)
    for n, column in enumerate(columns):
        block = jnp.where(lane == n, column, block)
    return block


def project_kernel(x_ref, gain_ref, wq_ref, wf_ref, wi_ref, wg_ref, out_ref):
    owners, rows, _ = out_ref.shape
    width = wq_ref.shape[-1]
    x = x_ref[...].reshape(owners * rows, x_ref.shape[-1]).astype(jnp.float32)
    squares = jnp.sum(x * x, axis=1, keepdims=True)
    power = exponent(squares)
    down = jnp.exp2(-power)
    factor = down * 2.0**13
    gained = (x * gain_ref[...].astype(jnp.float32)).astype(jnp.bfloat16)
    for n, w_ref in enumerate((wq_ref, wf_ref, wi_ref, wg_ref)):
        partial = jnp.dot(gained, w_ref[...], preferred_element_type=jnp.float32)
        out_ref[:, :, n * width : (n + 1) * width] = (factor * partial).reshape(owners, rows, width)
    mantissa = squares * down * down
    high = mantissa.astype(jnp.bfloat16).astype(jnp.float32)
    extra = lanes_of((power - 13.0, high, mantissa - high), owners * rows)
    out_ref[:, :, 4 * width :] = extra.reshape(owners, rows, EXTRA)


def project(whole, gain, weights, owners):
    rows = whole.shape[0] * whole.shape[1] // owners
    width = weights[0].shape[-1]
    return pl.pallas_call(
        project_kernel,
        out_shape=jax.ShapeDtypeStruct((owners, rows, 4 * width + EXTRA), jnp.float32),
        compiler_params=PARAMS,
        name="project",
    )(whole, gain, *weights)


def advance_kernel(block, parts_ref, shift_ref, bound_ref, gain_ref, prior_ref, *refs):
    new_ref, normed_ref, prior_s, new_s, in_sems, out_sems = refs[-6:]
    steps, _, _, size = prior_s.shape
    loads = [
        pltpu.make_async_copy(prior_ref.at[block, pl.ds(n * STEP, STEP), 0], prior_s.at[n], in_sems.at[n])
        for n in range(steps)
    ]
    stores = [
        pltpu.make_async_copy(new_s.at[n], new_ref.at[block, pl.ds(n * STEP, STEP), 0], out_sems.at[n])
        for n in range(steps)
    ]
    for load in loads:
        load.start()

    up = jnp.exp2(parts_ref[:, :, 4 * size : 4 * size + 1])
    mantissa = parts_ref[:, :, 4 * size + 1 : 4 * size + 2] + parts_ref[:, :, 4 * size + 2 : 4 * size + 3]
    whole = up * 2.0**13
    squares = jnp.sum(mantissa * whole * whole, axis=0)
    scale = lax.rsqrt(squares / D + epsilon)
    query, forget_in, value, gate = (
        scale * jnp.sum(parts_ref[:, :, n * size : (n + 1) * size] * up, axis=0) for n in range(4)
    )
    lower = jax.nn.sigmoid(bound_ref[...])
    pre = forget_in - shift_ref[...]
    forget = (lower + (1.0 - lower) * jax.nn.sigmoid(pre)).T
    key = ((1.0 - lower) * jax.nn.sigmoid(-pre)).T
    query = query.T
    gate = gain_ref[...] * (gate * jax.nn.sigmoid(gate))

    outs = []
    for n in range(steps):
        loads[n].wait()
        for m in range(STEP):
            at = slice(n * STEP + m, n * STEP + m + 1)
            updated = forget[:, at] * prior_s[n, m] + key[:, at] * value[at, :]
            new_s[n, m] = updated
            outs.append(jnp.sum(query[:, at] * updated, axis=0, keepdims=True))
        stores[n].start()
    readout = jnp.concatenate(outs, axis=0)
    mean = jnp.mean(readout * readout, axis=1, keepdims=True)
    normed = readout * lax.rsqrt(mean + epsilon) * gate
    normed_ref[...] = jnp.broadcast_to(normed.astype(jnp.bfloat16), normed_ref.shape)
    for store in stores:
        store.wait()


def advance(block, parts, shift, bound, gain_row, state, target):
    _, count, _, size, _ = state.shape
    owners = parts.shape[0]
    steps = count // STEP
    vmem, hbm = pl.BlockSpec(memory_space=pltpu.VMEM), pl.BlockSpec(memory_space=pltpu.HBM)
    extra = () if target is None else (target,)
    return pl.pallas_call(
        functools.partial(advance_kernel, block),
        in_specs=[vmem] * 4 + [hbm] * (1 + len(extra)),
        out_specs=[hbm, vmem],
        out_shape=[
            jax.ShapeDtypeStruct(state.shape, jnp.float32),
            jax.ShapeDtypeStruct((owners, count, size), jnp.bfloat16),
        ],
        scratch_shapes=[pltpu.VMEM((steps, STEP, size, size), jnp.float32)] * 2
        + [pltpu.SemaphoreType.DMA((steps,))] * 2,
        input_output_aliases={5: 0} if extra else {},
        compiler_params=PARAMS,
        name=f"advance{block}",
    )(parts, shift, bound, gain_row, state, *extra)


def branch_kernel(normed_ref, w_ref, out_ref):
    owners, rows, _ = out_ref.shape
    width = w_ref.shape[-1]
    normed = normed_ref[...].reshape(owners * rows, normed_ref.shape[-1])
    wide = normed.astype(jnp.float32)
    power = exponent(jnp.sum(wide * wide, axis=1, keepdims=True))
    total = jnp.dot(normed, w_ref[...], preferred_element_type=jnp.float32) * (jnp.exp2(-power) * 2.0**14)
    out_ref[:, :, :width] = total.reshape(owners, rows, width)
    out_ref[:, :, width:] = lanes_of((power - 14.0,), owners * rows).reshape(owners, rows, EXTRA)


def branch_parts(normed, weight, owners):
    rows = normed.shape[0] * normed.shape[1] // owners
    return pl.pallas_call(
        branch_kernel,
        out_shape=jax.ShapeDtypeStruct((owners, rows, weight.shape[1] + EXTRA), jnp.float32),
        compiler_params=PARAMS,
        name="branch",
    )(normed, weight)


def gathered(parts_ref):
    width = parts_ref.shape[-1] - EXTRA
    return jnp.sum(parts_ref[:, :, :width] * jnp.exp2(parts_ref[:, :, width : width + 1]), axis=0)


def next_kernel(parts_ref, x_ref, out_ref):
    x = (x_ref[...].astype(jnp.float32) + gathered(parts_ref)).astype(jnp.bfloat16)
    out_ref[...] = jnp.broadcast_to(x, out_ref.shape)


def final_kernel(parts_ref, x_ref, out_ref):
    out_ref[...] = x_ref[0].astype(jnp.float32) + gathered(parts_ref)


def shards(
    tokens,
    state,
    lengths,
    norm_gain,
    w_query,
    w_forget,
    w_input,
    w_gate,
    w_out,
    bound_logit,
    pace,
    head_gain,
):
    tp, dp = lax.axis_size("tp"), lax.axis_size("dp")
    log_len = jnp.log(lengths.astype(jnp.float32) / LENGTH_MEAN)
    copies = jnp.broadcast_to(tokens, (tp, *tokens.shape))
    target = None
    for block in range(2):
        whole = exchange(copies, "tp")
        weights = (w_query[block], w_forget[block], w_input[block], w_gate[block])
        parts = exchange_products(project(whole, norm_gain[block][None, :], weights, dp), "dp")
        shift = pace[block][None, :] * log_len[:, None]
        target, normed = advance(
            block, parts, shift, bound_logit[block][None, :], head_gain[block][None, :], state, target
        )
        parts = exchange_products(branch_parts(exchange(normed, "dp"), w_out[block], tp), "tp")
        if block == 0:
            copies = pl.pallas_call(
                next_kernel,
                out_shape=jax.ShapeDtypeStruct(copies.shape, jnp.bfloat16),
                compiler_params=PARAMS,
                name="next",
            )(parts, tokens)
        else:
            result = pl.pallas_call(
                final_kernel,
                out_shape=jax.ShapeDtypeStruct(tokens.shape, jnp.float32),
                compiler_params=PARAMS,
                name="final",
            )(parts, copies)
    return result, target


def solution(mesh):
    in_specs = (
        P(("grp", "tp"), "dp"),
        P(None, ("grp", "dp"), "tp", None, None),
        P(("grp", "dp")),
        P(None, "dp"),
        P(None, "dp", "tp"),
        P(None, "dp", "tp"),
        P(None, "dp", "tp"),
        P(None, "dp", "tp"),
        P(None, "tp", "dp"),
        P(None, "tp"),
        P(None, "tp"),
        P(),
    )
    out_specs = (P(("grp", "tp"), "dp"), P(None, ("grp", "dp"), "tp", None, None))
    return jax.shard_map(shards, mesh=mesh, in_specs=in_specs, out_specs=out_specs, check_vma=False)
```

time: 188 us -> 143 us (0.76)
  waiting for transfers between devices: 44.4 us -> 24.7 us
  matrix products: 16.4 us -> 0 us
  between operations: 14.5 us -> 0.8 us
  blocking collectives: 56.9 us -> 67 us
  Pallas kernels: 0 us -> 9.08 us
  other arithmetic: 10.6 us -> 1.74 us
  starting transfers between devices: 36.7 us -> 30.9 us
    dot_general x12 -> x0, matrix products: 16.4 us -> none  [the longest x2 8.41 us: advance(): jnp.einsum('bhk,bhkv->bhv', query.reshape(count, heads, size), updated, p...]
    all_gather x2 -> x0, waiting for transfers between devices: 12 us -> none  [sent_together(): result, at, done = (lax.all_gather(both, axis, axis=dim, tiled=True), 0, [])]
    all_to_all x4 -> x5, blocking collectives: 56.9 us -> 67 us  [exchange(): return lax.all_to_all(x, axis, split_axis=0, concat_axis=0, tiled=True)]
    pallas_call x0 -> x8, Pallas kernels: none -> 9.08 us  [the longest x2 7.34 us: advance(): pl.pallas_call(functools.partial(advance_kernel, block), in_specs=[vmem]...]
    all_to_all x4 -> x3, waiting for transfers between devices: 32.3 us -> 24.7 us  [exchange(): return lax.all_to_all(x, axis, split_axis=0, concat_axis=0, tiled=True)]
    all_to_all x4 -> x3, starting transfers between devices: 36.6 us -> 30.9 us  [exchange(): return lax.all_to_all(x, axis, split_axis=0, concat_axis=0, tiled=True)]
    add x2 -> x0, other arithmetic: 4.95 us -> none  [the longest x1 4.34 us: advance(): updated = forget[..., None] * prior + key[..., None] * values[:, :, None, :]]
    unnamed x22 -> x8, local copies, waits for them, and re-layouts: 5.11 us -> 2.19 us
  transfers between devices with their start and end apart: 6 -> 3, of which waited for: 5 -> 3; matrix products, arithmetic and copies ran while one was open for 11% -> 3% of each run, Pallas kernels for 0% -> 0%
where the time goes in v1:
time: 143 us; the launch traced here: 142 us
  blocking collectives  67 us (47%)
  starting transfers between devices  30.9 us (22%)
  waiting for transfers between devices  24.7 us (17%)
  Pallas kernels  9.08 us (6%)
  local copies, waits for them, and re-layouts  7.76 us (5%)
  other arithmetic  1.74 us (1%)
    all_to_all x5, blocking collectives, exchange(): return lax.all_to_all(x, axis, split_axis=0, concat_axis=0, tiled=True)  67 us
    all_to_all x3, starting transfers between devices, exchange(): return lax.all_to_all(x, axis, split_axis=0, concat_axis=0, tiled=True)  30.9 us
    all_to_all x3, waiting for transfers between devices, exchange(): return lax.all_to_all(x, axis, split_axis=0, concat_axis=0, tiled=True)  24.7 us
    pallas_call x2, Pallas kernels, advance(): pl.pallas_call(functools.partial(advance_kernel, block), in_specs=[vmem]...  7.34 us
  transfers between devices with their start and end apart: 3, of which 3 were waited for; matrix products, arithmetic and copies ran while one was open for 3% of the time, Pallas kernels for 0%

profile of v1, /device:TPU:513, one launch (start us, length us, event | category | flops | bytes accessed | tf_op | source)
XLA Modules:
  0.0 142.0 jit_solution(7078109755637442368)
XLA Ops:
  0.6 1.4 broadcast_in_dim.2
  2.0 23.7 %all-to-all-start = ((bf16[16,16,256]{2,1,0:T(8,128)(2,1)}), bf16[16,16,256]{2,1,0:T(8,128)(2,1)S(1)}, u32[]{:S(2)}, u32[]{:S(2)}) async-start(bf16[16,16,256]{2,1,0:T(8,128)(2,1)} %broadcast_in_dim.2), calls=%async_computation | async-start | bytes 262144 | tf_op jit(solution)/shard_map/all_to_all | solution.py:21
  25.7 0.8 fusion.2
  26.5 1.0 slice_bitcast_fusion.3
  27.4 0.8 slice_bitcast_fusion.10
  28.2 1.0 slice_bitcast_fusion.1
  29.1 5.8 %all-to-all-done.x_ref = bf16[16,16,256]{2,1,0:T(8,128)(2,1)S(1)} async-done(((bf16[16,16,256]{2,1,0:T(8,128)(2,1)}), bf16[16,16,256]{2,1,0:T(8,128)(2,1)S(1)}, u32[]{:S(2)}, u32[]{:S(2)}) %all-to-all-start) | async-done | bytes 131104 | tf_op jit(solution)/shard_map/all_to_all | solution.py:21
  35.0 0.0 copy-start.3
  35.0 0.3 project.2
  35.3 0.8 convert_element_type.27
  36.0 3.6 %all-to-all-start.1 = ((f16[8,32,640]{2,1,0:T(8,128)(2,1)}), f16[8,32,640]{2,1,0:T(8,128)(2,1)S(1)}, u32[]{:S(2)}, u32[]{:S(2)}) async-start(f16[8,32,640]{2,1,0:T(8,128)(2,1)} %convert_element_type.27), calls=%async_computation.1 | async-start | bytes 655360 | tf_op jit(solution)/shard_map/all_to_all | solution.py:21
  39.7 0.7 multiply_log_fusion
  40.3 0.8 fusion
  41.1 0.0 copy-start.2
  41.1 0.1 broadcast_multiply_fusion
  41.2 12.0 %all-to-all-done.1 = f16[8,32,640]{2,1,0:T(8,128)(2,1)S(1)} async-done(((f16[8,32,640]{2,1,0:T(8,128)(2,1)}), f16[8,32,640]{2,1,0:T(8,128)(2,1)S(1)}, u32[]{:S(2)}, u32[]{:S(2)}) %all-to-all-start.1) | async-done | bytes 327712 | tf_op jit(solution)/shard_map/all_to_all | solution.py:21
  53.3 0.0 copy-start
  53.3 2.2 %copy-done = f32[2,32,1,128,128]{4,3,2,1,0:T(8,128)S(1)} copy-done((f32[2,32,1,128,128]{4,3,2,1,0:T(8,128)S(1)}, f32[2,32,1,128,128]{4,3,2,1,0:T(8,128)}, u32[]{:S(2)}) %copy-start) | copy-done | bytes 4194328
  55.4 4.0 %advance0.1 = (f32[2,32,1,128,128]{4,3,2,1,0:T(8,128)}, bf16[8,32,128]{2,1,0:T(8,128)(2,1)}) custom-call(f32[8,32,640]{2,1,0:T(8,128)S(1)} %convert_element_type.28.parts_ref, f32[32,128]{1,0:T(8,128)S(1)} %get-tuple-element.29.shift_ref, f32[1,128]{1,0:T(1,128)S(1)} %get-tuple-element.34.bound_ref, f32[1,128]{1,0:T(1,128)S(1)} %get-tuple-element.21.gain_ref, ...), custom_call_target="tpu_custom_call" | custom-call | tf_op jit(solution)/shard_map/advance0/pallas_call | solution.py:121
  59.4 3.6 %all-to-all-start.2 = ((bf16[8,32,128]{2,1,0:T(8,128)(2,1)}), bf16[8,32,128]{2,1,0:T(8,128)(2,1)S(1)}, u32[]{:S(2)}, u32[]{:S(2)}) async-start(bf16[8,32,128]{2,1,0:T(8,128)(2,1)} %get-tuple-element.6), calls=%async_computation.2 | async-start | bytes 131072 | tf_op jit(solution)/shard_map/all_to_all | solution.py:21
  63.0 0.0 copy-done.3
  63.0 6.9 %all-to-all-done.2.normed_ref = bf16[8,32,128]{2,1,0:T(8,128)(2,1)S(1)} async-done(((bf16[8,32,128]{2,1,0:T(8,128)(2,1)}), bf16[8,32,128]{2,1,0:T(8,128)(2,1)S(1)}, u32[]{:S(2)}, u32[]{:S(2)}) %all-to-all-start.2) | async-done | bytes 65568 | tf_op jit(solution)/shard_map/all_to_all | solution.py:21
  69.9 0.0 copy-start.1
  69.9 0.2 branch.2
  70.1 15.1 %all_to_all.40 = f16[16,16,384]{2,1,0:T(8,128)(2,1)S(1)} all-to-all(f16[16,16,384]{2,1,0:T(8,128)(2,1)S(1)} %convert_element_type.30), channel_id=1, replica_groups=mesh['grp'=2,'tp'=16,'dp'=8] {'tp'}, dimensions={0} | all-to-all | bytes 393216 | tf_op jit(solution)/shard_map/all_to_all | solution.py:21
  85.2 0.0 copy-done.2
  85.2 0.1 next.1.x_ref
  85.4 11.4 %all_to_all.41.x_ref = bf16[16,16,256]{2,1,0:T(8,128)(2,1)S(1)} all-to-all(bf16[16,16,256]{2,1,0:T(8,128)(2,1)S(1)} %next.1.x_ref), channel_id=1, replica_groups=mesh['grp'=2,'tp'=16,'dp'=8] {'tp'}, dimensions={0} | all-to-all | bytes 262144 | tf_op jit(solution)/shard_map/all_to_all | solution.py:21
  96.7 0.3 project.3
  97.1 15.5 %all_to_all.42 = f16[8,32,640]{2,1,0:T(8,128)(2,1)S(1)} all-to-all(f16[8,32,640]{2,1,0:T(8,128)(2,1)S(1)} %convert_element_type.32), channel_id=1, replica_groups=mesh['grp'=2,'tp'=16,'dp'=8] {'dp'}, dimensions={0} | all-to-all | bytes 655360 | tf_op jit(solution)/shard_map/all_to_all | solution.py:21
  112.6 0.0 copy-done.1
  112.6 3.4 %advance1.1 = (f32[2,32,1,128,128]{4,3,2,1,0:T(8,128)}, bf16[8,32,128]{2,1,0:T(8,128)(2,1)S(1)}) custom-call(f32[8,32,640]{2,1,0:T(8,128)S(1)} %convert_element_type.33.parts_ref, f32[32,128]{1,0:T(8,128)S(1)} %get-tuple-element.28.shift_ref, f32[1,128]{1,0:T(1,128)S(1)} %get-tuple-element.35.bound_ref, ...), custom_call_target="tpu_custom_call", output_to_operand_aliasing={{0}: (5, {})} | custom-call | tf_op jit(solution)/shard_map/advance1/pallas_call | solution.py:121
  116.0 9.6 %all_to_all.43.normed_ref = bf16[8,32,128]{2,1,0:T(8,128)(2,1)S(1)} all-to-all(bf16[8,32,128]{2,1,0:T(8,128)(2,1)S(1)} %get-tuple-element.8), channel_id=1, replica_groups=mesh['grp'=2,'tp'=16,'dp'=8] {'dp'}, dimensions={0} | all-to-all | bytes 131072 | tf_op jit(solution)/shard_map/all_to_all | solution.py:21
  125.6 0.2 branch.3
  125.9 15.4 %all_to_all.44 = f16[16,16,384]{2,1,0:T(8,128)(2,1)S(1)} all-to-all(f16[16,16,384]{2,1,0:T(8,128)(2,1)S(1)} %convert_element_type.34), channel_id=1, replica_groups=mesh['grp'=2,'tp'=16,'dp'=8] {'tp'}, dimensions={0} | all-to-all | bytes 393216 | tf_op jit(solution)/shard_map/all_to_all | solution.py:21
  141.3 0.7 final.1
  (8 shorter events, 0.3 us)
Async XLA Ops:
  2.0 33.0 %all-to-all-start = ((bf16[16,16,256]{2,1,0:T(8,128)(2,1)}), bf16[16,16,256]{2,1,0:T(8,128)(2,1)S(1)}, u32[]{:S(2)}, u32[]{:S(2)}) async-start(bf16[16,16,256]{2,1,0:T(8,128)(2,1)} %broadcast_in_dim.2), calls=%async_computation | async-start | bytes 262144 | tf_op jit(solution)/shard_map/all_to_all | solution.py:21
  35.0 28.0 %copy-start.3 = (bf16[2,128,256]{2,1,0:T(8,128)(2,1)S(1)}, bf16[2,128,256]{2,1,0:T(8,128)(2,1)}, u32[]{:S(2)}) copy-start(bf16[2,128,256]{2,1,0:T(8,128)(2,1)} %param.20) | copy-start | bytes 393220
  36.0 17.2 %all-to-all-start.1 = ((f16[8,32,640]{2,1,0:T(8,128)(2,1)}), f16[8,32,640]{2,1,0:T(8,128)(2,1)S(1)}, u32[]{:S(2)}, u32[]{:S(2)}) async-start(f16[8,32,640]{2,1,0:T(8,128)(2,1)} %convert_element_type.27), calls=%async_computation.1 | async-start | bytes 655360 | tf_op jit(solution)/shard_map/all_to_all | solution.py:21
  41.1 44.1 %copy-start.2 = (bf16[16,256]{1,0:T(8,128)(2,1)S(1)}, bf16[16,256]{1,0:T(8,128)(2,1)}, u32[]{:S(2)}) copy-start(bf16[16,256]{1,0:T(8,128)(2,1)} %x_ref.1) | copy-start | bytes 24580
  53.3 2.2 %copy-start = (f32[2,32,1,128,128]{4,3,2,1,0:T(8,128)S(1)}, f32[2,32,1,128,128]{4,3,2,1,0:T(8,128)}, u32[]{:S(2)}) copy-start(f32[2,32,1,128,128]{4,3,2,1,0:T(8,128)} %prior_ref.3) | copy-start | bytes 12582916
  59.4 10.5 %all-to-all-start.2 = ((bf16[8,32,128]{2,1,0:T(8,128)(2,1)}), bf16[8,32,128]{2,1,0:T(8,128)(2,1)S(1)}, u32[]{:S(2)}, u32[]{:S(2)}) async-start(bf16[8,32,128]{2,1,0:T(8,128)(2,1)} %get-tuple-element.6), calls=%async_computation.2 | async-start | bytes 131072 | tf_op jit(solution)/shard_map/all_to_all | solution.py:21
  69.9 42.7 %copy-start.1 = (f32[2,32,1,128,128]{4,3,2,1,0:T(8,128)S(1)}, f32[2,32,1,128,128]{4,3,2,1,0:T(8,128)}, u32[]{:S(2)}) copy-start(f32[2,32,1,128,128]{4,3,2,1,0:T(8,128)} %prior_ref.3) | copy-start | bytes 12582916

commit v2 on v1

v2 whole, which is shorter than its diff:
```python
import functools

import jax
import jax.numpy as jnp
from jax import lax
from jax.experimental import pallas as pl
from jax.experimental.pallas import tpu as pltpu
from jax.sharding import PartitionSpec as P

D = 2048
LENGTH_MEAN = 512
FLOOR = 2.0**-80
EXTRA = 8
STEP = 8
PARAMS = pltpu.CompilerParams(vmem_limit_bytes=16 << 20)
WIDE_PARAMS = pltpu.CompilerParams(vmem_limit_bytes=51 << 20)
PREP_PARAMS = pltpu.CompilerParams(vmem_limit_bytes=54900 << 10)
VMEM = pl.BlockSpec(memory_space=pltpu.VMEM)
HBM = pl.BlockSpec(memory_space=pltpu.HBM)

epsilon = 1e-06


def exchange(x, axis):
    return lax.all_to_all(x, axis, split_axis=0, concat_axis=0, tiled=True)


def exchange_products(x, axis):
    return exchange(x.astype(jnp.float16), axis).astype(jnp.float32)


def prep_kernel(lengths_ref, pace_ref, gain_ref, bound_ref, head_ref, *refs):
    weights, shift_ref, rows, firsts, sems = refs[:4], refs[4], refs[5:8], refs[8:12], refs[12]
    copies = [pltpu.make_async_copy(w_ref.at[0], first, sems.at[n]) for n, (w_ref, first) in enumerate(zip(weights, firsts))]
    for copy in copies:
        copy.start()
    count = shift_ref.shape[1]
    log_len = jnp.log(lengths_ref[...].astype(jnp.float32) / LENGTH_MEAN)
    across = lax.broadcasted_iota(jnp.int32, (count, count), 0) == lax.broadcasted_iota(jnp.int32, (count, count), 1)
    column = jnp.sum(jnp.where(across, jnp.broadcast_to(log_len, (count, count)), 0.0), axis=1, keepdims=True)
    for block in range(shift_ref.shape[0]):
        shift_ref[block] = pace_ref[block : block + 1, :] * column
    for row, ref in zip(rows, (gain_ref, bound_ref, head_ref)):
        row[...] = ref[...].astype(jnp.float32)
    for copy in copies:
        copy.wait()


def prep(lengths, pace, rows, weights):
    blocks, size = pace.shape
    out = pl.pallas_call(
        prep_kernel,
        in_specs=[VMEM] * (2 + len(rows)) + [HBM] * len(weights),
        out_specs=[VMEM] * (1 + len(rows) + len(weights)),
        out_shape=[jax.ShapeDtypeStruct((blocks, *lengths.shape, size), jnp.float32)]
        + [jax.ShapeDtypeStruct(row.shape, jnp.float32) for row in rows]
        + [jax.ShapeDtypeStruct(w.shape[1:], w.dtype) for w in weights],
        scratch_shapes=[pltpu.SemaphoreType.DMA((len(weights),))],
        compiler_params=PREP_PARAMS,
        name="prep",
    )(lengths[None, :], pace, *rows, *weights)
    return out[0], out[1 : 1 + len(rows)], out[1 + len(rows) :]


def project_kernel(block, x_ref, gain_ref, wq_ref, wf_ref, wi_ref, wg_ref, out_ref):
    owners, size = out_ref.shape[0], out_ref.shape[-1]
    rows = (out_ref.shape[1] - EXTRA) // 4
    x = x_ref[...].reshape(owners * rows, x_ref.shape[-1]).astype(jnp.float32)
    squares = jnp.sum(x * x, axis=1, keepdims=True)
    power = jnp.ceil(0.5 * jnp.log2(jnp.maximum(squares, FLOOR)))
    down = jnp.exp2(-power)
    factor = down * 2.0**13
    gained = (x * gain_ref[block : block + 1, :]).astype(jnp.bfloat16)
    for n, w_ref in enumerate((wq_ref, wf_ref, wi_ref, wg_ref)):
        weight = w_ref[block] if len(w_ref.shape) == 3 else w_ref[...]
        partial = jnp.dot(gained, weight, preferred_element_type=jnp.float32)
        out_ref[:, n * rows : (n + 1) * rows, :] = (factor * partial).reshape(owners, rows, size)
    mantissa = squares * down * down
    high = mantissa.astype(jnp.bfloat16).astype(jnp.float32)
    lane = lax.broadcasted_iota(jnp.int32, (owners * rows, size), 1)
    table = jnp.where(lane == 0, power - 13.0, jnp.where(lane == 1, high, jnp.where(lane == 2, mantissa - high, 0.0)))
    table = table.T[:EXTRA, :]
    for owner in range(owners):
        window = owner * rows // size * size
        turned = table[:, window : window + size]
        if owner * rows > window:
            turned = pltpu.roll(turned, size - (owner * rows - window), 1)
        out_ref[owner, 4 * rows :, :] = turned


def project(block, whole, gain, weights, owners):
    rows = whole.shape[0] * whole.shape[1] // owners
    width = weights[0].shape[-1]
    return pl.pallas_call(
        functools.partial(project_kernel, block),
        out_shape=jax.ShapeDtypeStruct((owners, 4 * rows + EXTRA, width), jnp.float32),
        compiler_params=PARAMS,
        name="project",
    )(whole, gain, *weights)


def advance_kernel(block, parts_ref, shift_ref, bound_ref, gain_ref, prior_ref, *refs):
    new_ref, normed_ref, prior_s, new_s, in_sems, out_sems = refs[-6:]
    steps = prior_s.shape[0]
    owners, count, size = normed_ref.shape
    loads = [
        pltpu.make_async_copy(prior_ref.at[block, pl.ds(n * STEP, STEP), 0], prior_s.at[n], in_sems.at[n])
        for n in range(steps)
    ]
    stores = [
        pltpu.make_async_copy(new_s.at[n], new_ref.at[block, pl.ds(n * STEP, STEP), 0], out_sems.at[n])
        for n in range(steps)
    ]
    for load in loads:
        load.start()

    up = jnp.exp2(parts_ref[:, 4 * count, :].T[:count, :])
    mantissa = (parts_ref[:, 4 * count + 1, :] + parts_ref[:, 4 * count + 2, :]).T[:count, :]
    norms = up * 2.0**13
    squares = jnp.sum(mantissa * norms * norms, axis=1, keepdims=True)
    scale = lax.rsqrt(squares / D + epsilon)

    def whole(n):
        total = parts_ref[0, n * count : (n + 1) * count, :] * up[:, 0:1]
        for source in range(1, owners):
            total += parts_ref[source, n * count : (n + 1) * count, :] * up[:, source : source + 1]
        return scale * total

    query, forget_in, value, gate = (whole(n) for n in range(4))
    lower = jax.nn.sigmoid(bound_ref[block : block + 1, :])
    pre = forget_in - shift_ref[block]
    forget = (lower + (1.0 - lower) * jax.nn.sigmoid(pre)).T
    key = ((1.0 - lower) * jax.nn.sigmoid(-pre)).T
    query = query.T
    gate = gain_ref[block : block + 1, :] * (gate * jax.nn.sigmoid(gate))

    outs = []
    for n in range(steps):
        loads[n].wait()
        for m in range(STEP):
            at = slice(n * STEP + m, n * STEP + m + 1)
            updated = forget[:, at] * prior_s[n, m] + key[:, at] * value[at, :]
            new_s[n, m] = updated
            outs.append(jnp.sum(query[:, at] * updated, axis=0, keepdims=True))
        stores[n].start()
    readout = jnp.concatenate(outs, axis=0)
    mean = jnp.mean(readout * readout, axis=1, keepdims=True)
    normed = readout * lax.rsqrt(mean + epsilon) * gate
    normed_ref[...] = jnp.broadcast_to(normed.astype(jnp.bfloat16), normed_ref.shape)
    for store in stores:
        store.wait()


def advance(block, parts, shift, bound, gain_row, state, target):
    _, count, _, size, _ = state.shape
    steps = count // STEP
    extra = () if target is None else (target,)
    return pl.pallas_call(
        functools.partial(advance_kernel, block),
        in_specs=[VMEM] * 4 + [HBM] * (1 + len(extra)),
        out_specs=[HBM, VMEM],
        out_shape=[
            jax.ShapeDtypeStruct(state.shape, jnp.float32),
            jax.ShapeDtypeStruct((parts.shape[0], count, size), jnp.bfloat16),
        ],
        scratch_shapes=[pltpu.VMEM((steps, STEP, size, size), jnp.float32)] * 2
        + [pltpu.SemaphoreType.DMA((steps,))] * 2,
        input_output_aliases={5: 0} if extra else {},
        compiler_params=WIDE_PARAMS,
        name="advance",
    )(parts, shift, bound, gain_row, state, *extra)


def branch_kernel(block, normed_ref, w_ref, out_ref):
    normed = normed_ref[...].reshape(-1, normed_ref.shape[-1])
    total = jnp.dot(normed, w_ref[block], preferred_element_type=jnp.float32)
    root = jnp.sqrt(jnp.abs(total)) * 2.0**8
    out_ref[...] = jnp.where(total < 0.0, -root, root).reshape(out_ref.shape)


def branch_parts(block, normed, weight, owners):
    rows = normed.shape[0] * normed.shape[1] // owners
    return pl.pallas_call(
        functools.partial(branch_kernel, block),
        out_shape=jax.ShapeDtypeStruct((owners, rows, weight.shape[2]), jnp.float32),
        compiler_params=PARAMS,
        name="branch",
    )(normed, weight)


def gathered(parts_ref):
    parts = parts_ref[...]
    return jnp.sum(parts * jnp.abs(parts), axis=0) * 2.0**-16


def next_kernel(parts_ref, x_ref, out_ref):
    x = (x_ref[...].astype(jnp.float32) + gathered(parts_ref)).astype(jnp.bfloat16)
    out_ref[...] = jnp.broadcast_to(x, out_ref.shape)


def final_kernel(parts_ref, x_ref, out_ref):
    out_ref[...] = x_ref[0].astype(jnp.float32) + gathered(parts_ref)


def shards(
    tokens,
    state,
    lengths,
    norm_gain,
    w_query,
    w_forget,
    w_input,
    w_gate,
    w_out,
    bound_logit,
    pace,
    head_gain,
):
    tp, dp = lax.axis_size("tp"), lax.axis_size("dp")
    copies = jnp.broadcast_to(tokens, (tp, *tokens.shape))
    weights = (w_query, w_forget, w_input, w_gate)
    shift, (norm_gain, bound_logit, head_gain), firsts = prep(lengths, pace, (norm_gain, bound_logit, head_gain), weights)
    target = None
    for block in range(2):
        whole = exchange(copies, "tp")
        parts = exchange_products(project(block, whole, norm_gain, weights if block else firsts, dp), "dp")
        target, normed = advance(block, parts, shift, bound_logit, head_gain, state, target)
        parts = exchange_products(branch_parts(block, exchange(normed, "dp"), w_out, tp), "tp")
        if block == 0:
            copies = pl.pallas_call(
                next_kernel,
                out_shape=jax.ShapeDtypeStruct(copies.shape, jnp.bfloat16),
                compiler_params=PARAMS,
                name="next",
            )(parts, tokens)
        else:
            result = pl.pallas_call(
                final_kernel,
                out_shape=jax.ShapeDtypeStruct(tokens.shape, jnp.float32),
                compiler_params=PARAMS,
                name="final",
            )(parts, copies)
    return result, target


def solution(mesh):
    in_specs = (
        P(("grp", "tp"), "dp"),
        P(None, ("grp", "dp"), "tp", None, None),
        P(("grp", "dp")),
        P(None, "dp"),
        P(None, "dp", "tp"),
        P(None, "dp", "tp"),
        P(None, "dp", "tp"),
        P(None, "dp", "tp"),
        P(None, "tp", "dp"),
        P(None, "tp"),
        P(None, "tp"),
        P(),
    )
    out_specs = (P(("grp", "tp"), "dp"), P(None, ("grp", "dp"), "tp", None, None))
    return jax.shard_map(shards, mesh=mesh, in_specs=in_specs, out_specs=out_specs, check_vma=False)
```

time: 143 us -> 134 us (0.937)
  blocking collectives: 67 us -> 87.7 us
  waiting for transfers between devices: 24.7 us -> 4.87 us
  starting transfers between devices: 30.9 us -> 23.7 us
  local copies, waits for them, and re-layouts: 7.76 us -> 4.76 us
  Pallas kernels: 9.08 us -> 10.8 us
  other arithmetic: 1.74 us -> 0.24 us
    all_to_all x5 -> x7, blocking collectives: 67 us -> 87.7 us  [exchange(): return lax.all_to_all(x, axis, split_axis=0, concat_axis=0, tiled=True)]
    all_to_all x3 -> x1, waiting for transfers between devices: 24.7 us -> 4.87 us  [exchange(): return lax.all_to_all(x, axis, split_axis=0, concat_axis=0, tiled=True)]
    all_to_all x3 -> x1, starting transfers between devices: 30.9 us -> 23.7 us  [exchange(): return lax.all_to_all(x, axis, split_axis=0, concat_axis=0, tiled=True)]
    squeeze x3 -> x0, local copies, waits for them, and re-layouts: 1.92 us -> none  [the longest x2 1.9 us: shards(): weights = (w_query[block], w_forget[block], w_input[block], w_gate[block])]
    pallas_call x6 -> x7, Pallas kernels: 8.25 us -> 10.1 us  [the longest x2 8.02 us: advance(): pl.pallas_call(functools.partial(advance_kernel, block), in_specs=[VMEM]...]
    slice x2 -> x0, local copies, waits for them, and re-layouts: 1.52 us -> none  [the longest x1 0.77 us: shards(): head_gain[block][None, :]]
    unnamed x8 -> x22, local copies, waits for them, and re-layouts: 2.19 us -> 3.4 us
  transfers between devices with their start and end apart: 3 -> 1, of which waited for: 3 -> 1; matrix products, arithmetic and copies ran while one was open for 3% -> 0% of each run, Pallas kernels for 0% -> 1%
where the time goes in v2:
time: 134 us; the launch traced here: 133 us
  blocking collectives  87.7 us (65%)
  starting transfers between devices  23.7 us (18%)
  Pallas kernels  10.8 us (8%)
  waiting for transfers between devices  4.87 us (4%)
  local copies, waits for them, and re-layouts  4.76 us (4%)
    all_to_all x7, blocking collectives, exchange(): return lax.all_to_all(x, axis, split_axis=0, concat_axis=0, tiled=True)  87.7 us
    all_to_all x1, starting transfers between devices, exchange(): return lax.all_to_all(x, axis, split_axis=0, concat_axis=0, tiled=True)  23.7 us
    pallas_call x2, Pallas kernels, advance(): pl.pallas_call(functools.partial(advance_kernel, block), in_specs=[VMEM]...  8.02 us
    all_to_all x1, waiting for transfers between devices, exchange(): return lax.all_to_all(x, axis, split_axis=0, concat_axis=0, tiled=True)  4.87 us
    unnamed x22, local copies, waits for them, and re-layouts  3.4 us
  transfers between devices with their start and end apart: 1, of which 1 were waited for; matrix products, arithmetic and copies ran while one was open for 0% of the time, Pallas kernels for 1%

profile of v2, /device:TPU:513, one launch (start us, length us, event | category | flops | bytes accessed | tf_op | source)
XLA Modules:
  0.0 132.9 jit_solution(6360626002291508434)
XLA Ops:
  0.6 1.4 %broadcast_in_dim.6 = bf16[16,16,256]{2,1,0:T(8,128)(2,1)} broadcast(bf16[16,256]{1,0:T(8,128)(2,1)} %x_ref.1), dimensions={1,2} | broadcast | bytes 139264 | tf_op jit(solution)/shard_map/broadcast_in_dim | solution.py:220
  2.0 23.7 %all-to-all-start = ((bf16[16,16,256]{2,1,0:T(8,128)(2,1)}), bf16[16,16,256]{2,1,0:T(8,128)(2,1)S(1)}, u32[]{:S(2)}, u32[]{:S(2)}) async-start(bf16[16,16,256]{2,1,0:T(8,128)(2,1)} %broadcast_in_dim.6), calls=%async_computation | async-start | bytes 262144 | tf_op jit(solution)/shard_map/all_to_all | solution.py:25
  25.7 0.0 copy-start.6
  25.7 0.7 copy-done.6
  26.4 0.0 copy-start.7
  26.4 0.7 copy-done.7
  27.1 0.0 copy-start.8
  27.1 0.7 copy-done.8
  27.8 0.0 copy-start.9
  27.8 0.7 copy-done.9
  28.4 0.0 copy-start.10
  28.4 0.7 copy-done.10
  29.1 0.0 copy-start.4
  29.1 1.0 prep.1
  30.1 4.9 %all-to-all-done.x_ref = bf16[16,16,256]{2,1,0:T(8,128)(2,1)S(1)} async-done(((bf16[16,16,256]{2,1,0:T(8,128)(2,1)}), bf16[16,16,256]{2,1,0:T(8,128)(2,1)S(1)}, u32[]{:S(2)}, u32[]{:S(2)}) %all-to-all-start) | async-done | bytes 131104 | tf_op jit(solution)/shard_map/all_to_all | solution.py:25
  35.0 0.3 project.2
  35.3 0.0 copy-start.5
  35.3 0.0 copy-start
  35.3 0.0 copy-start.1
  35.4 0.0 copy-start.2
  35.4 0.0 copy-start.3
  35.4 15.3 %all_to_all.40 = f16[8,136,128]{2,1,0:T(8,128)(2,1)S(1)} all-to-all(f16[8,136,128]{2,1,0:T(8,128)(2,1)S(1)} %convert_element_type.24), channel_id=1, replica_groups=mesh['grp'=2,'tp'=16,'dp'=8] {'dp'}, dimensions={0} | all-to-all | bytes 557056 | tf_op jit(solution)/shard_map/all_to_all | solution.py:25
  50.7 4.1 %advance.2 = (f32[2,32,1,128,128]{4,3,2,1,0:T(8,128)}, bf16[8,32,128]{2,1,0:T(8,128)(2,1)S(1)}) custom-call(f32[8,136,128]{2,1,0:T(8,128)S(1)} %convert_element_type.25.parts_ref, f32[2,32,128]{2,1,0:T(8,128)S(1)} %get-tuple-element.19.shift_ref, f32[2,128]{1,0:T(2,128)S(1)} %get-tuple-element.20.bound_ref, f32[2,128]{1,0:T(2,128)S(1)} %get-tuple-element.21.gain_ref, ...), custom_call_target="tpu_custom_call" | custom-call | tf_op jit(solution)/shard_map/advance/pallas_call | solution.py:158
  54.8 9.6 %all_to_all.41.normed_ref = bf16[8,32,128]{2,1,0:T(8,128)(2,1)S(1)} all-to-all(bf16[8,32,128]{2,1,0:T(8,128)(2,1)S(1)} %get-tuple-element.22), channel_id=1, replica_groups=mesh['grp'=2,'tp'=16,'dp'=8] {'dp'}, dimensions={0} | all-to-all | bytes 131072 | tf_op jit(solution)/shard_map/all_to_all | solution.py:25
  64.4 0.0 copy-done.4
  64.4 0.2 branch.2
  64.7 13.4 %all_to_all.42 = f16[16,16,256]{2,1,0:T(8,128)(2,1)S(1)} all-to-all(f16[16,16,256]{2,1,0:T(8,128)(2,1)S(1)} %convert_element_type.26), channel_id=1, replica_groups=mesh['grp'=2,'tp'=16,'dp'=8] {'tp'}, dimensions={0} | all-to-all | bytes 262144 | tf_op jit(solution)/shard_map/all_to_all | solution.py:25
  78.2 0.0 copy-done.5
  78.2 11.3 %all_to_all.43.x_ref = bf16[16,16,256]{2,1,0:T(8,128)(2,1)S(1)} all-to-all(bf16[16,16,256]{2,1,0:T(8,128)(2,1)S(1)} %next.1.x_ref), channel_id=1, replica_groups=mesh['grp'=2,'tp'=16,'dp'=8] {'tp'}, dimensions={0} | all-to-all | bytes 262144 | tf_op jit(solution)/shard_map/all_to_all | solution.py:25
  89.5 0.0 copy-done
  89.5 0.0 copy-done.1
  89.6 0.0 copy-done.2
  89.6 0.0 copy-done.3
  89.6 0.3 project.3
  89.9 15.1 %all_to_all.44 = f16[8,136,128]{2,1,0:T(8,128)(2,1)S(1)} all-to-all(f16[8,136,128]{2,1,0:T(8,128)(2,1)S(1)} %convert_element_type.28), channel_id=1, replica_groups=mesh['grp'=2,'tp'=16,'dp'=8] {'dp'}, dimensions={0} | all-to-all | bytes 557056 | tf_op jit(solution)/shard_map/all_to_all | solution.py:25
  105.1 3.9 %advance.3 = (f32[2,32,1,128,128]{4,3,2,1,0:T(8,128)}, bf16[8,32,128]{2,1,0:T(8,128)(2,1)S(1)}) custom-call(f32[8,136,128]{2,1,0:T(8,128)S(1)} %convert_element_type.29.parts_ref, f32[2,32,128]{2,1,0:T(8,128)S(1)} %get-tuple-element.19.shift_ref, f32[2,128]{1,0:T(2,128)S(1)} %get-tuple-element.20.bound_ref, ...), custom_call_target="tpu_custom_call", output_to_operand_aliasing={{0}: (5, {})} | custom-call | tf_op jit(solution)/shard_map/advance/pallas_call | solution.py:158
  108.9 9.6 %all_to_all.45.normed_ref = bf16[8,32,128]{2,1,0:T(8,128)(2,1)S(1)} all-to-all(bf16[8,32,128]{2,1,0:T(8,128)(2,1)S(1)} %get-tuple-element.24), channel_id=1, replica_groups=mesh['grp'=2,'tp'=16,'dp'=8] {'dp'}, dimensions={0} | all-to-all | bytes 131072 | tf_op jit(solution)/shard_map/all_to_all | solution.py:25
  118.5 0.2 branch.3
  118.8 13.4 %all_to_all.46 = f16[16,16,256]{2,1,0:T(8,128)(2,1)S(1)} all-to-all(f16[16,16,256]{2,1,0:T(8,128)(2,1)S(1)} %convert_element_type.30), channel_id=1, replica_groups=mesh['grp'=2,'tp'=16,'dp'=8] {'tp'}, dimensions={0} | all-to-all | bytes 262144 | tf_op jit(solution)/shard_map/all_to_all | solution.py:25
  132.3 0.6 final.1
  (9 shorter events, 0.3 us)
Async XLA Ops:
  2.0 33.0 %all-to-all-start = ((bf16[16,16,256]{2,1,0:T(8,128)(2,1)}), bf16[16,16,256]{2,1,0:T(8,128)(2,1)S(1)}, u32[]{:S(2)}, u32[]{:S(2)}) async-start(bf16[16,16,256]{2,1,0:T(8,128)(2,1)} %broadcast_in_dim.6), calls=%async_computation | async-start | bytes 262144 | tf_op jit(solution)/shard_map/all_to_all | solution.py:25
  25.7 0.7 copy-start.6
  26.4 0.7 copy-start.7
  27.1 0.7 copy-start.8
  27.8 0.7 copy-start.9
  28.4 0.7 copy-start.10
  29.1 35.3 %copy-start.4 = (bf16[2,128,256]{2,1,0:T(8,128)(2,1)S(1)}, bf16[2,128,256]{2,1,0:T(8,128)(2,1)}, u32[]{:S(2)}) copy-start(bf16[2,128,256]{2,1,0:T(8,128)(2,1)} %w_ref.3) | copy-start | bytes 393220
  35.3 42.9 %copy-start.5 = (bf16[16,256]{1,0:T(8,128)(2,1)S(1)}, bf16[16,256]{1,0:T(8,128)(2,1)}, u32[]{:S(2)}) copy-start(bf16[16,256]{1,0:T(8,128)(2,1)} %x_ref.1) | copy-start | bytes 24580
  35.3 54.2 %copy-start = (bf16[2,256,128]{2,1,0:T(8,128)(2,1)S(1)}, bf16[2,256,128]{2,1,0:T(8,128)(2,1)}, u32[]{:S(2)}) copy-start(bf16[2,256,128]{2,1,0:T(8,128)(2,1)} %wq_ref.1) | copy-start | bytes 393220
  35.3 54.2 %copy-start.1 = (bf16[2,256,128]{2,1,0:T(8,128)(2,1)S(1)}, bf16[2,256,128]{2,1,0:T(8,128)(2,1)}, u32[]{:S(2)}) copy-start(bf16[2,256,128]{2,1,0:T(8,128)(2,1)} %wf_ref.1) | copy-start | bytes 393220
  35.4 54.2 %copy-start.2 = (bf16[2,256,128]{2,1,0:T(8,128)(2,1)S(1)}, bf16[2,256,128]{2,1,0:T(8,128)(2,1)}, u32[]{:S(2)}) copy-start(bf16[2,256,128]{2,1,0:T(8,128)(2,1)} %wi_ref.1) | copy-start | bytes 393220
  35.4 54.2 %copy-start.3 = (bf16[2,256,128]{2,1,0:T(8,128)(2,1)S(1)}, bf16[2,256,128]{2,1,0:T(8,128)(2,1)}, u32[]{:S(2)}) copy-start(bf16[2,256,128]{2,1,0:T(8,128)(2,1)} %wg_ref.1) | copy-start | bytes 393220

commit v3 on v2

v3 whole, which is shorter than its diff:
```python
import functools

import jax
import jax.numpy as jnp
from jax import lax
from jax.experimental import pallas as pl
from jax.experimental.pallas import tpu as pltpu
from jax.sharding import PartitionSpec as P

D = 2048
LENGTH_MEAN = 512
FLOOR = 2.0**-80
PAD = 16
SHARE_AT = 16
STEP = 8
PARAMS = pltpu.CompilerParams(vmem_limit_bytes=16 << 20)
WIDE_PARAMS = pltpu.CompilerParams(vmem_limit_bytes=51 << 20)
SECOND_PARAMS = pltpu.CompilerParams(vmem_limit_bytes=49 << 20)
PACK_PARAMS = pltpu.CompilerParams(vmem_limit_bytes=54900 << 10)
VMEM = pl.BlockSpec(memory_space=pltpu.VMEM)
HBM = pl.BlockSpec(memory_space=pltpu.HBM)

epsilon = 1e-06


def exchange(x, axis):
    return lax.all_to_all(x, axis, split_axis=0, concat_axis=0, tiled=True)


def exchange_products(x, axis):
    return exchange(x.astype(jnp.float16), axis).astype(jnp.float32)


def pack_kernel(block, gain_ref, wq_ref, wf_ref, wi_ref, wg_ref, out_ref, sems):
    rows, size = wq_ref.shape[1:]
    copies = [
        pltpu.make_async_copy(w_ref.at[block], out_ref.at[pl.ds(0, rows), pl.ds(n * size, size)], sems.at[n])
        for n, w_ref in enumerate((wq_ref, wf_ref, wi_ref, wg_ref))
    ]
    for copy in copies:
        copy.start()
    gain = jnp.broadcast_to(gain_ref[block : block + 1, :].astype(jnp.float32), (PAD, rows))
    out_ref[rows:, :rows] = gain.astype(out_ref.dtype)
    out_ref[rows:, rows:] = jnp.zeros((PAD, 4 * size - rows), out_ref.dtype)
    for copy in copies:
        copy.wait()


def pack(block, gain, weights):
    _, rows, size = weights[0].shape
    return pl.pallas_call(
        functools.partial(pack_kernel, block),
        in_specs=[VMEM] + [HBM] * 4,
        out_specs=VMEM,
        out_shape=jax.ShapeDtypeStruct((rows + PAD, 4 * size), jnp.bfloat16),
        scratch_shapes=[pltpu.SemaphoreType.DMA((4,))],
        compiler_params=PACK_PARAMS,
        name="pack",
    )(gain, *weights)


def around(shard, axis):
    size = lax.axis_size(axis)
    onward = [(n, (n + 1) % size) for n in range(size)]
    back = [(n, (n - 1) % size) for n in range(size)]
    held = {0: shard}
    for step in range(1, size // 2 + 1):
        held[size - step] = lax.ppermute(held[(size - step + 1) % size], axis, onward)
        if step < size // 2:
            held[step] = lax.ppermute(held[step - 1], axis, back)
    return [held[n] for n in range(size)]


def selection(wide, narrow, first, share, transposed):
    shape = (narrow, wide) if transposed else (wide, narrow)
    long = lax.broadcasted_iota(jnp.int32, shape, 1 if transposed else 0)
    short = lax.broadcasted_iota(jnp.int32, shape, 0 if transposed else 1) - first
    inside = (short >= 0) & (short < share) & (long == lax.axis_index("tp") * share + short)
    return jnp.where(inside, 1.0, 0.0).astype(jnp.bfloat16)


def code(total):
    root = jnp.sqrt(jnp.abs(total)) * 2.0**6
    return jnp.where(total < 0.0, -root, root)


def project_kernel(share, x_ref, w_ref, out_ref):
    owners, size = out_ref.shape[0], out_ref.shape[-1]
    rows = out_ref.shape[1] // 5
    held = x_ref[...].reshape(owners * rows, x_ref.shape[-1])
    x = held.astype(jnp.float32)
    squares = jnp.sum(x * x, axis=1, keepdims=True)
    power = jnp.ceil(0.5 * jnp.log2(jnp.maximum(squares, FLOOR)))
    down = jnp.exp2(-power)
    factor = down * 2.0**13
    features = x.shape[1]
    gained = (x * w_ref[features : features + 1, :features].astype(jnp.float32)).astype(jnp.bfloat16)
    partial = factor * jnp.dot(gained, w_ref[:features, :], preferred_element_type=jnp.float32)
    for n in range(4):
        out_ref[:, n * rows : (n + 1) * rows, :] = partial[:, n * size : (n + 1) * size].reshape(owners, rows, size)
    mantissa = squares * down * down
    high = mantissa.astype(jnp.bfloat16).astype(jnp.float32)
    lane = lax.broadcasted_iota(jnp.int32, (owners * rows, size), 1)
    table = jnp.where(lane == 0, power - 13.0, jnp.where(lane == 1, high, jnp.where(lane == 2, mantissa - high, 0.0)))
    choose = selection(held.shape[1], size, SHARE_AT, share, False)
    kept = factor * jnp.dot(held, choose, preferred_element_type=jnp.float32)
    out_ref[:, 4 * rows :, :] = (table + kept).reshape(owners, rows, size)


def project(whole, weight, owners):
    rows = whole.shape[0] * whole.shape[1] // owners
    share = whole.shape[2] // lax.axis_size("tp")
    return pl.pallas_call(
        functools.partial(project_kernel, share),
        out_shape=jax.ShapeDtypeStruct((owners, 5 * rows, weight.shape[1] // 4), jnp.float32),
        compiler_params=PARAMS,
        name="project",
    )(whole, weight)


def moves(block, state_ref, new_ref, prior_s, new_s, in_sems, out_sems):
    steps = prior_s.shape[0]
    rows = [pl.ds(n * STEP, STEP) for n in range(steps)]
    loads = [pltpu.make_async_copy(state_ref.at[block, rows[n], 0], prior_s.at[n], in_sems.at[n]) for n in range(steps)]
    stores = [pltpu.make_async_copy(new_s.at[n], new_ref.at[block, rows[n], 0], out_sems.at[n]) for n in range(steps)]
    return loads, stores


def recur(block, made, shift_ref, bound_ref, head_ref, loads, stores, prior_s, new_s):
    query, forget_in, value, gate = made
    lower = jax.nn.sigmoid(bound_ref[block : block + 1, :])
    pre = forget_in - shift_ref[block]
    forget = (lower + (1.0 - lower) * jax.nn.sigmoid(pre)).T
    key = ((1.0 - lower) * jax.nn.sigmoid(-pre)).T
    query = query.T
    gate = head_ref[block : block + 1, :] * (gate * jax.nn.sigmoid(gate))
    outs = []
    for n in range(len(loads)):
        loads[n].wait()
        for m in range(STEP):
            at = slice(n * STEP + m, n * STEP + m + 1)
            updated = forget[:, at] * prior_s[n, m] + key[:, at] * value[at, :]
            new_s[n, m] = updated
            outs.append(jnp.sum(query[:, at] * updated, axis=0, keepdims=True))
        stores[n].start()
    readout = jnp.concatenate(outs, axis=0)
    mean = jnp.mean(readout * readout, axis=1, keepdims=True)
    return (readout * lax.rsqrt(mean + epsilon) * gate).astype(jnp.bfloat16)


def first_kernel(share, parts_ref, shift_ref, bound_ref, head_ref, *refs):
    shards, (state_ref, new_ref, out_ref, *scratch) = refs[:-7], refs[-7:]
    loads, stores = moves(0, state_ref, new_ref, *scratch)
    for load in loads:
        load.start()
    owners, _, size = parts_ref.shape
    count = out_ref.shape[1]
    made, squares = [0.0] * 4, 0.0
    for source in range(owners):
        table = parts_ref[source, 4 * count :, :]
        up = jnp.exp2(table[:, 0:1])
        norm = up * 2.0**13
        squares += (table[:, 1:2] + table[:, 2:3]) * norm * norm
        for n in range(4):
            made[n] += parts_ref[source, n * count : (n + 1) * count, :] * up
    scale = lax.rsqrt(squares / D + epsilon)
    made = [scale * total for total in made]
    normed = recur(0, made, shift_ref, bound_ref, head_ref, loads, stores, *scratch[:2])
    width = shards[0].shape[1]
    place = selection(width, size, SHARE_AT, share, True)
    for n, shard in enumerate(shards):
        chunk = lax.rem(lax.axis_index("dp") + n, owners)
        table = parts_ref[chunk, 4 * count :, :]
        branch = jnp.dot(normed, shard[...], preferred_element_type=jnp.float32)
        kept = jnp.dot(table.astype(jnp.bfloat16), place, preferred_element_type=jnp.float32)
        coded = code(branch + jnp.exp2(table[:, 0:1]) * kept)
        for part in range(width // size):
            out_ref[chunk * (width // size) + part] = coded[:, part * size : (part + 1) * size]
    for store in stores:
        store.wait()


def scratch_of(state):
    _, count, _, size, _ = state.shape
    steps = count // STEP
    return [pltpu.VMEM((steps, STEP, size, size), jnp.float32)] * 2 + [pltpu.SemaphoreType.DMA((steps,))] * 2


def first(parts, shift, bound, head, shards, state):
    _, count, _, size, _ = state.shape
    tp = lax.axis_size("tp")
    return pl.pallas_call(
        functools.partial(first_kernel, shards[0].shape[1] // tp),
        in_specs=[VMEM] * (4 + len(shards)) + [HBM],
        out_specs=[HBM, VMEM],
        out_shape=[
            jax.ShapeDtypeStruct(state.shape, jnp.float32),
            jax.ShapeDtypeStruct((tp, count, size), jnp.float32),
        ],
        scratch_shapes=scratch_of(state),
        compiler_params=WIDE_PARAMS,
        name="first",
    )(parts, shift, bound, head, *shards, state)


def decoded(parts_ref):
    parts = parts_ref[...]
    return jnp.sum(parts * jnp.abs(parts), axis=0) * 2.0**-12


def next_kernel(parts_ref, out_ref):
    out_ref[...] = jnp.broadcast_to(decoded(parts_ref).astype(jnp.bfloat16), out_ref.shape)


def second_kernel(share, x_ref, shift_ref, bound_ref, head_ref, *refs):
    shards, (state_ref, _, new_ref, out_ref, *scratch) = refs[:-8], refs[-8:]
    loads, stores = moves(1, state_ref, new_ref, *scratch)
    for load in loads:
        load.start()
    owners, _, size = out_ref.shape
    rows = shards[0].shape[0] - PAD
    parts = rows // size
    count = x_ref.shape[1]
    choose = selection(rows, size, 0, share, False)
    made, squares = 0.0, 0.0
    for n, shard in enumerate(shards):
        chunk = lax.rem(lax.axis_index("dp") + n, owners)
        held = jnp.concatenate([x_ref[chunk * parts + part] for part in range(parts)], axis=1)
        wide = held.astype(jnp.float32)
        squares += jnp.sum(wide * wide, axis=1, keepdims=True)
        gained = (wide * shard[rows : rows + 1, :rows].astype(jnp.float32)).astype(jnp.bfloat16)
        made += jnp.dot(gained, shard[:rows, :], preferred_element_type=jnp.float32)
        kept = jnp.dot(held, choose, preferred_element_type=jnp.float32)
        out_ref[chunk, count:, :] = kept.astype(jnp.bfloat16)
    made = lax.rsqrt(squares / D + epsilon) * made
    made = [made[:, n * size : (n + 1) * size] for n in range(4)]
    normed = recur(1, made, shift_ref, bound_ref, head_ref, loads, stores, *scratch[:2])
    out_ref[:, :count, :] = jnp.broadcast_to(normed, (owners, count, size))
    for store in stores:
        store.wait()


def second(x, shift, bound, head, shards, state, target):
    _, count, _, size, _ = state.shape
    rows = shards[0].shape[0] - PAD
    return pl.pallas_call(
        functools.partial(second_kernel, rows // lax.axis_size("tp")),
        in_specs=[VMEM] * (4 + len(shards)) + [HBM] * 2,
        out_specs=[HBM, VMEM],
        out_shape=[
            jax.ShapeDtypeStruct(state.shape, jnp.float32),
            jax.ShapeDtypeStruct((len(shards), 2 * count, size), jnp.bfloat16),
        ],
        scratch_shapes=scratch_of(state),
        input_output_aliases={5 + len(shards): 0},
        compiler_params=SECOND_PARAMS,
        name="second",
    )(x, shift, bound, head, *shards, state, target)


def branch_kernel(share, normed_ref, w_ref, out_ref):
    count, size = normed_ref.shape[1] // 2, normed_ref.shape[2]
    normed = normed_ref[:, :count, :].reshape(-1, size)
    held = normed_ref[:, count:, :].reshape(-1, size)
    weight = w_ref[1]
    total = jnp.dot(normed, weight, preferred_element_type=jnp.float32)
    place = selection(weight.shape[1], size, 0, share, True)
    total += jnp.dot(held, place, preferred_element_type=jnp.float32)
    out_ref[...] = code(total).reshape(out_ref.shape)


def branch_parts(normed, weight, owners):
    rows = normed.shape[0] * normed.shape[1] // 2 // owners
    return pl.pallas_call(
        functools.partial(branch_kernel, weight.shape[2] // owners),
        out_shape=jax.ShapeDtypeStruct((owners, rows, weight.shape[2]), jnp.float32),
        compiler_params=PARAMS,
        name="branch",
    )(normed, weight)


def final_kernel(parts_ref, out_ref):
    out_ref[...] = decoded(parts_ref)


def shards(
    tokens,
    state,
    lengths,
    norm_gain,
    w_query,
    w_forget,
    w_input,
    w_gate,
    w_out,
    bound_logit,
    pace,
    head_gain,
):
    tp, dp = lax.axis_size("tp"), lax.axis_size("dp")
    whole = exchange(jnp.broadcast_to(tokens, (tp, *tokens.shape)), "tp")
    weights = (w_query, w_forget, w_input, w_gate)
    back = around(w_out[0], "dp")
    weight = pack(0, norm_gain, weights)
    held = around(pack(1, norm_gain, weights), "dp")
    log_len = jnp.log(lengths.astype(jnp.float32) / LENGTH_MEAN)
    shift = pace[:, None, :] * log_len[None, :, None]

    parts = exchange_products(project(whole, weight, dp), "dp")
    target, parts = first(parts, shift, bound_logit, head_gain, back, state)
    parts = exchange_products(parts, "tp")
    copies = pl.pallas_call(
        next_kernel,
        out_shape=jax.ShapeDtypeStruct(parts.shape, jnp.bfloat16),
        compiler_params=PARAMS,
        name="next",
    )(parts)
    target, normed = second(exchange(copies, "tp"), shift, bound_logit, head_gain, held, state, target)
    parts = exchange_products(branch_parts(exchange(normed, "dp"), w_out, tp), "tp")
    result = pl.pallas_call(
        final_kernel,
        out_shape=jax.ShapeDtypeStruct(tokens.shape, jnp.float32),
        compiler_params=PARAMS,
        name="final",
    )(parts)
    return result, target


def solution(mesh):
    in_specs = (
        P(("grp", "tp"), "dp"),
        P(None, ("grp", "dp"), "tp", None, None),
        P(("grp", "dp")),
        P(None, "dp"),
        P(None, "dp", "tp"),
        P(None, "dp", "tp"),
        P(None, "dp", "tp"),
        P(None, "dp", "tp"),
        P(None, "tp", "dp"),
        P(None, "tp"),
        P(None, "tp"),
        P(),
    )
    out_specs = (P(("grp", "tp"), "dp"), P(None, ("grp", "dp"), "tp", None, None))
    return jax.shard_map(shards, mesh=mesh, in_specs=in_specs, out_specs=out_specs, check_vma=False)
```

time: 134 us -> 134 us (level)
  blocking collectives: 87.7 us -> 28 us
  starting transfers between devices: 23.7 us -> 53.1 us
  waiting for transfers between devices: 4.87 us -> 30.2 us
  Pallas kernels: 10.8 us -> 13.3 us
  other arithmetic: 0.24 us -> 1.62 us
    all_to_all x7 -> x2, blocking collectives: 87.7 us -> 28 us  [exchange(): return lax.all_to_all(x, axis, split_axis=0, concat_axis=0, tiled=True)]
    all_to_all x1 -> x4, starting transfers between devices: 23.7 us -> 40.1 us  [exchange(): return lax.all_to_all(x, axis, split_axis=0, concat_axis=0, tiled=True)]
    all_to_all x1 -> x4, waiting for transfers between devices: 4.87 us -> 18.5 us  [exchange(): return lax.all_to_all(x, axis, split_axis=0, concat_axis=0, tiled=True)]
    ppermute x0 -> x14, starting transfers between devices: none -> 13.1 us  [the longest x6 12.2 us: around(): held[step] = lax.ppermute(held[step - 1], axis, back)]
    ppermute x0 -> x14, waiting for transfers between devices: none -> 11.7 us  [the longest x6 10.2 us: around(): held[step] = lax.ppermute(held[step - 1], axis, back)]
    pallas_call x8 -> x7, Pallas kernels: 10.1 us -> 12.7 us  [the longest x1 4.15 us: second(): pl.pallas_call(functools.partial(second_kernel, rows // lax.axis_size('tp...]
    unnamed x22 -> x20, local copies, waits for them, and re-layouts: 3.4 us -> 3.46 us
  transfers between devices with their start and end apart: 1 -> 18, of which waited for: 1 -> 6; matrix products, arithmetic and copies ran while one was open for 0% -> 2% of each run, Pallas kernels for 1% -> 6%
where the time goes in v3:
time: 134 us; the launch traced here: 133 us
  starting transfers between devices  53.1 us (40%)
  waiting for transfers between devices  30.2 us (23%)
  blocking collectives  28 us (21%)
  Pallas kernels  13.3 us (10%)
  local copies, waits for them, and re-layouts  5.68 us (4%)
  other arithmetic  1.62 us (1%)
    all_to_all x4, starting transfers between devices, exchange(): return lax.all_to_all(x, axis, split_axis=0, concat_axis=0, tiled=True)  40.1 us
    all_to_all x2, blocking collectives, exchange(): return lax.all_to_all(x, axis, split_axis=0, concat_axis=0, tiled=True)  28 us
    all_to_all x4, waiting for transfers between devices, exchange(): return lax.all_to_all(x, axis, split_axis=0, concat_axis=0, tiled=True)  18.5 us
    ppermute x6, starting transfers between devices, around(): held[step] = lax.ppermute(held[step - 1], axis, back)  12.2 us
    ppermute x6, waiting for transfers between devices, around(): held[step] = lax.ppermute(held[step - 1], axis, back)  10.2 us
    pallas_call x1, Pallas kernels, second(): pl.pallas_call(functools.partial(second_kernel, rows // lax.axis_size('tp...  4.15 us
    pallas_call x1, Pallas kernels, first(): pl.pallas_call(functools.partial(first_kernel, shards[0].shape[1] // tp),...  4.06 us
    unnamed x20, local copies, waits for them, and re-layouts  3.46 us
  transfers between devices with their start and end apart: 18, of which 6 were waited for; matrix products, arithmetic and copies ran while one was open for 2% of the time, Pallas kernels for 6%

profile of v3, /device:TPU:513, one launch (start us, length us, event | category | flops | bytes accessed | tf_op | source)
XLA Modules:
  0.0 132.8 jit_solution(8596949013473067400)
XLA Ops:
  0.7 1.4 %broadcast_in_dim.2 = bf16[16,16,256]{2,1,0:T(8,128)(2,1)} broadcast(bf16[16,256]{1,0:T(8,128)(2,1)} %param.12), dimensions={1,2} | broadcast | bytes 139264 | tf_op jit(solution)/shard_map/broadcast_in_dim | solution.py:301
  2.0 23.7 %all-to-all-start = ((bf16[16,16,256]{2,1,0:T(8,128)(2,1)}), bf16[16,16,256]{2,1,0:T(8,128)(2,1)S(1)}, u32[]{:S(2)}, u32[]{:S(2)}) async-start(bf16[16,16,256]{2,1,0:T(8,128)(2,1)} %broadcast_in_dim.2), calls=%async_computation | async-start | bytes 262144 | tf_op jit(solution)/shard_map/all_to_all | solution.py:27
  25.8 0.9 copy-done.2
  26.7 0.9 copy-done.3
  27.6 0.7 copy-done.5
  28.3 1.6 %pack.3.refs_0_ = bf16[272,512]{1,0:T(8,128)(2,1)} custom-call(bf16[2,256]{1,0:T(2,128)(2,1)S(1)} %copy-done.5, bf16[2,256,128]{2,1,0:T(8,128)(2,1)S(1)} %copy-done.2, bf16[2,256,128]{2,1,0:T(8,128)(2,1)S(1)} %copy-done.3, bf16[2,256,128]{2,1,0:T(8,128)(2,1)} %wi_ref.3, bf16[2,256,128]{2,1,0:T(8,128)(2,1)} %wg_ref.3), custom_call_target="tpu_custom_call" | custom-call | tf_op jit(solution)/shard_map/pack/pallas_call | solution.py:51
  29.9 0.1 collective-permute-start.10
  30.0 0.8 slice_bitcast_fusion.refs_0_
  30.9 0.0 collective-permute-start.3
  30.9 1.6 %pack.2.w_ref = bf16[272,512]{1,0:T(8,128)(2,1)} custom-call(bf16[2,256]{1,0:T(2,128)(2,1)S(1)} %copy-done.5, bf16[2,256,128]{2,1,0:T(8,128)(2,1)S(1)} %copy-done.2, bf16[2,256,128]{2,1,0:T(8,128)(2,1)S(1)} %copy-done.3, bf16[2,256,128]{2,1,0:T(8,128)(2,1)} %wi_ref.3, bf16[2,256,128]{2,1,0:T(8,128)(2,1)} %wg_ref.3), custom_call_target="tpu_custom_call" | custom-call | tf_op jit(solution)/shard_map/pack/pallas_call | solution.py:51
  32.5 2.5 %all-to-all-done.x_ref = bf16[16,16,256]{2,1,0:T(8,128)(2,1)S(1)} async-done(((bf16[16,16,256]{2,1,0:T(8,128)(2,1)}), bf16[16,16,256]{2,1,0:T(8,128)(2,1)S(1)}, u32[]{:S(2)}, u32[]{:S(2)}) %all-to-all-start) | async-done | bytes 131104 | tf_op jit(solution)/shard_map/all_to_all | solution.py:27
  35.0 1.0 copy-done.1
  36.0 0.3 project.1
  36.3 0.8 convert_element_type.21
  37.0 3.6 %all-to-all-start.1 = ((f16[8,160,128]{2,1,0:T(8,128)(2,1)}), f16[8,160,128]{2,1,0:T(8,128)(2,1)S(1)}, u32[]{:S(2)}, u32[]{:S(2)}) async-start(f16[8,160,128]{2,1,0:T(8,128)(2,1)} %convert_element_type.21), calls=%async_computation.1 | async-start | bytes 655360 | tf_op jit(solution)/shard_map/all_to_all | solution.py:27
  40.7 2.5 %collective-permute-start = (bf16[128,256]{1,0:T(8,128)(2,1)S(1)}, bf16[128,256]{1,0:T(8,128)(2,1)S(1)}, u32[]{:S(2)}, u32[]{:S(2)}) collective-permute-start(bf16[128,256]{1,0:T(8,128)(2,1)S(1)} %slice_bitcast_fusion.refs_0_), channel_id=1, source_target_pairs={{0,7},{1,0},{2,1},{3,2},{4,3},{5,4},{6,5},{7,6},{8,15},{9,8},{10,9... | collective-permute-start | bytes 196616 | tf_op jit(solution)/shard_map/ppermute | solution.py:70
  43.2 0.0 collective-permute-done.3.refs_7_
  43.2 2.7 %collective-permute-start.7 = (bf16[272,512]{1,0:T(8,128)(2,1)}, bf16[272,512]{1,0:T(8,128)(2,1)S(1)}, u32[]{:S(2)}, u32[]{:S(2)}) collective-permute-start(bf16[272,512]{1,0:T(8,128)(2,1)} %pack.3.refs_0_), channel_id=1, source_target_pairs={{0,7},{1,0},{2,1},{3,2},{4,3},{5,4},{6,5},{7,6},{8,15},{9,8},{10,9... | collective-permute-start | bytes 835592 | tf_op jit(solution)/shard_map/ppermute | solution.py:70
  45.9 3.6 %collective-permute-done.refs_1_ = bf16[128,256]{1,0:T(8,128)(2,1)S(1)} collective-permute-done((bf16[128,256]{1,0:T(8,128)(2,1)S(1)}, bf16[128,256]{1,0:T(8,128)(2,1)S(1)}, u32[]{:S(2)}, u32[]{:S(2)}) %collective-permute-start) | collective-permute-done | bytes 65568 | tf_op jit(solution)/shard_map/ppermute | solution.py:70
  49.4 1.8 %collective-permute-start.1 = (bf16[128,256]{1,0:T(8,128)(2,1)S(1)}, bf16[128,256]{1,0:T(8,128)(2,1)S(1)}, u32[]{:S(2)}, u32[]{:S(2)}) collective-permute-start(bf16[128,256]{1,0:T(8,128)(2,1)S(1)} %collective-permute-done.refs_1_), channel_id=1, source_target_pairs={{0,7},{1,0},{2,1},{3,2},{4,3},{5,4},{6,5},{7,6},{8,15},{9,8},{10,9... | collective-permute-start | bytes 196616 | tf_op jit(solution)/shard_map/ppermute | solution.py:70
  51.2 0.0 collective-permute-done.4.refs_6_
  51.2 0.0 collective-permute-start.5
  51.2 6.6 %collective-permute-done.1.refs_2_ = bf16[128,256]{1,0:T(8,128)(2,1)S(1)} collective-permute-done((bf16[128,256]{1,0:T(8,128)(2,1)S(1)}, bf16[128,256]{1,0:T(8,128)(2,1)S(1)}, u32[]{:S(2)}, u32[]{:S(2)}) %collective-permute-start.1) | collective-permute-done | bytes 65568 | tf_op jit(solution)/shard_map/ppermute | solution.py:70
  57.8 1.8 %collective-permute-start.2 = (bf16[128,256]{1,0:T(8,128)(2,1)S(1)}, bf16[128,256]{1,0:T(8,128)(2,1)S(1)}, u32[]{:S(2)}, u32[]{:S(2)}) collective-permute-start(bf16[128,256]{1,0:T(8,128)(2,1)S(1)} %collective-permute-done.1.refs_2_), channel_id=1, source_target_pairs={{0,7},{1,0},{2,1},{3,2},{4,3},{5,4},{6,5},{7,6},{8,15},{9,8},{10,9... | collective-permute-start | bytes 196616 | tf_op jit(solution)/shard_map/ppermute | solution.py:70
  59.6 0.0 collective-permute-start.6
  59.6 0.0 collective-permute-done.7.refs_1_
  59.6 2.7 %collective-permute-start.8 = (bf16[272,512]{1,0:T(8,128)(2,1)S(1)}, bf16[272,512]{1,0:T(8,128)(2,1)S(1)}, u32[]{:S(2)}, u32[]{:S(2)}) collective-permute-start(bf16[272,512]{1,0:T(8,128)(2,1)S(1)} %collective-permute-done.7.refs_1_), channel_id=1, source_target_pairs={{0,7},{1,0},{2,1},{3,2},{4,3},{5,4},{6,5},{7,6},{8,15},{9,8},{10,9... | collective-permute-start | bytes 835592 | tf_op jit(solution)/shard_map/ppermute | solution.py:70
  62.3 0.0 collective-permute-done.11.refs_6_
  62.3 0.0 collective-permute-start.12
  62.3 0.1 broadcast_multiply_fusion.shift_ref
  62.4 1.5 %collective-permute-done.6.refs_4_ = bf16[128,256]{1,0:T(8,128)(2,1)S(1)} collective-permute-done((bf16[128,256]{1,0:T(8,128)(2,1)S(1)}, bf16[128,256]{1,0:T(8,128)(2,1)S(1)}, u32[]{:S(2)}, u32[]{:S(2)}) %collective-permute-start.6) | collective-permute-done | bytes 65568 | tf_op jit(solution)/shard_map/ppermute | solution.py:68
  64.0 4.1 %first.1 = (f32[2,32,1,128,128]{4,3,2,1,0:T(8,128)}, f32[16,32,128]{2,1,0:T(8,128)S(1)}) custom-call(f32[8,160,128]{2,1,0:T(8,128)S(1)} %convert_element_type.22.parts_ref, f32[2,32,128]{2,1,0:T(8,128)S(1)} %broadcast_multiply_fusion.shift_ref, f32[2,128]{1,0:T(2,128)S(1)} %copy-done.6, f32[2,128]{1,0:T(2,128)S(1)} %copy-done.7, ...), custom_call_target="tpu_custom_call" | custom-call | tf_op jit(solution)/shard_map/first/pallas_call | solution.py:192
  68.0 0.7 convert_element_type.24
  68.7 9.0 %all-to-all-start.2 = ((f16[16,32,128]{2,1,0:T(8,128)(2,1)}), f16[16,32,128]{2,1,0:T(8,128)(2,1)S(1)}, u32[]{:S(2)}, u32[]{:S(2)}) async-start(f16[16,32,128]{2,1,0:T(8,128)(2,1)} %convert_element_type.24), calls=%async_computation.2 | async-start | bytes 262144 | tf_op jit(solution)/shard_map/all_to_all | solution.py:27
  77.7 0.9 collective-permute-start.9
  78.6 0.0 collective-permute-done.12.refs_5_
  78.6 0.7 collective-permute-start.13
  79.3 7.3 %all-to-all-done.2 = f16[16,32,128]{2,1,0:T(8,128)(2,1)S(1)} async-done(((f16[16,32,128]{2,1,0:T(8,128)(2,1)}), f16[16,32,128]{2,1,0:T(8,128)(2,1)S(1)}, u32[]{:S(2)}, u32[]{:S(2)}) %all-to-all-start.2) | async-done | bytes 131104 | tf_op jit(solution)/shard_map/all_to_all | solution.py:27
  86.6 0.7 next.1
  87.3 3.7 %all-to-all-start.3 = ((bf16[16,32,128]{2,1,0:T(8,128)(2,1)}), bf16[16,32,128]{2,1,0:T(8,128)(2,1)S(1)}, u32[]{:S(2)}, u32[]{:S(2)}) async-start(bf16[16,32,128]{2,1,0:T(8,128)(2,1)} %next.1), calls=%async_computation.3 | async-start | bytes 262144 | tf_op jit(solution)/shard_map/all_to_all | solution.py:27
  91.0 0.0 collective-permute-done.9.refs_3_
  91.0 0.0 collective-permute-done.13.refs_4_
  91.0 8.7 %all-to-all-done.3.x_ref = bf16[16,32,128]{2,1,0:T(8,128)(2,1)S(1)} async-done(((bf16[16,32,128]{2,1,0:T(8,128)(2,1)}), bf16[16,32,128]{2,1,0:T(8,128)(2,1)S(1)}, u32[]{:S(2)}, u32[]{:S(2)}) %all-to-all-start.3) | async-done | bytes 131104 | tf_op jit(solution)/shard_map/all_to_all | solution.py:27
  99.7 4.1 %second.1 = (f32[2,32,1,128,128]{4,3,2,1,0:T(8,128)}, bf16[8,64,128]{2,1,0:T(8,128)(2,1)S(1)}) custom-call(bf16[16,32,128]{2,1,0:T(8,128)(2,1)S(1)} %all-to-all-done.3.x_ref, f32[2,32,128]{2,1,0:T(8,128)S(1)} %broadcast_multiply_fusion.shift_ref, f32[2,128]{1,0:T(2,128)S(1)} %copy-done.6, f32[2,128]{1,0:T(2,128)S(1)} %copy-done.7, ...), custom_call_target="tpu_custom_call", output_to_operand_aliasing={{0}: (13, {})} | custom-call | tf_op jit(solution)/shard_map/second/pallas_call | solution.py:246
  103.9 15.8 %all_to_all.30.normed_ref = bf16[8,64,128]{2,1,0:T(8,128)(2,1)S(1)} all-to-all(bf16[8,64,128]{2,1,0:T(8,128)(2,1)S(1)} %get-tuple-element.8), channel_id=1, replica_groups=mesh['grp'=2,'tp'=16,'dp'=8] {'dp'}, dimensions={0} | all-to-all | bytes 262144 | tf_op jit(solution)/shard_map/all_to_all | solution.py:27
  119.7 0.3 branch.1
  120.0 12.2 %all_to_all.31 = f16[16,16,256]{2,1,0:T(8,128)(2,1)S(1)} all-to-all(f16[16,16,256]{2,1,0:T(8,128)(2,1)S(1)} %convert_element_type.26), channel_id=1, replica_groups=mesh['grp'=2,'tp'=16,'dp'=8] {'tp'}, dimensions={0} | all-to-all | bytes 262144 | tf_op jit(solution)/shard_map/all_to_all | solution.py:27
  132.2 0.6 final.1
  (28 shorter events, 0.2 us)
Async XLA Ops:
  0.6 50.6 %copy-start.9 = (s32[32]{0:T(128)S(1)}, s32[32]{0:T(128)}, u32[]{:S(2)}) copy-start(s32[32]{0:T(128)} %param.14) | copy-start | bytes 388
  0.6 61.7 %copy-start.8 = (f32[2,128]{1,0:T(2,128)S(1)}, f32[2,128]{1,0:T(2,128)}, u32[]{:S(2)}) copy-start(f32[2,128]{1,0:T(2,128)} %param.22) | copy-start | bytes 3076
  0.7 63.3 %copy-start.7 = (f32[2,128]{1,0:T(2,128)S(1)}, f32[2,128]{1,0:T(2,128)}, u32[]{:S(2)}) copy-start(f32[2,128]{1,0:T(2,128)} %head_ref.3) | copy-start | bytes 3076
  0.7 63.3 %copy-start.6 = (f32[2,128]{1,0:T(2,128)S(1)}, f32[2,128]{1,0:T(2,128)}, u32[]{:S(2)}) copy-start(f32[2,128]{1,0:T(2,128)} %bound_ref.3) | copy-start | bytes 3076
  2.0 33.0 %all-to-all-start = ((bf16[16,16,256]{2,1,0:T(8,128)(2,1)}), bf16[16,16,256]{2,1,0:T(8,128)(2,1)S(1)}, u32[]{:S(2)}, u32[]{:S(2)}) async-start(bf16[16,16,256]{2,1,0:T(8,128)(2,1)} %broadcast_in_dim.2), calls=%async_computation | async-start | bytes 262144 | tf_op jit(solution)/shard_map/all_to_all | solution.py:27
  25.8 0.9 copy-start.2
  26.7 0.9 copy-start.3
  27.6 0.7 copy-start.5
  29.9 16.0 %collective-permute-start.10 = (bf16[272,512]{1,0:T(8,128)(2,1)}, bf16[272,512]{1,0:T(8,128)(2,1)S(1)}, u32[]{:S(2)}, u32[]{:S(2)}) collective-permute-start(bf16[272,512]{1,0:T(8,128)(2,1)} %pack.3.refs_0_), channel_id=1, source_target_pairs={{0,1},{1,2},{2,3},{3,4},{4,5},{5,6},{6,7},{7,0},{8,9},{9,10},{10,1... | collective-permute-start | bytes 835592 | tf_op jit(solution)/shard_map/ppermute | solution.py:68
  30.9 12.3 %collective-permute-start.3 = (bf16[128,256]{1,0:T(8,128)(2,1)S(1)}, bf16[128,256]{1,0:T(8,128)(2,1)S(1)}, u32[]{:S(2)}, u32[]{:S(2)}) collective-permute-start(bf16[128,256]{1,0:T(8,128)(2,1)S(1)} %slice_bitcast_fusion.refs_0_), channel_id=1, source_target_pairs={{0,1},{1,2},{2,3},{3,4},{4,5},{5,6},{6,7},{7,0},{8,9},{9,10},{10,1... | collective-permute-start | bytes 196616 | tf_op jit(solution)/shard_map/ppermute | solution.py:68
  35.0 1.0 copy-start.1
  37.0 25.4 %all-to-all-start.1 = ((f16[8,160,128]{2,1,0:T(8,128)(2,1)}), f16[8,160,128]{2,1,0:T(8,128)(2,1)S(1)}, u32[]{:S(2)}, u32[]{:S(2)}) async-start(f16[8,160,128]{2,1,0:T(8,128)(2,1)} %convert_element_type.21), calls=%async_computation.1 | async-start | bytes 655360 | tf_op jit(solution)/shard_map/all_to_all | solution.py:27
  40.7 59.1 %copy-start = (bf16[272,512]{1,0:T(8,128)(2,1)S(1)}, bf16[272,512]{1,0:T(8,128)(2,1)}, u32[]{:S(2)}) copy-start(bf16[272,512]{1,0:T(8,128)(2,1)} %pack.3.refs_0_) | copy-start | bytes 835588
  40.7 8.8 %collective-permute-start = (bf16[128,256]{1,0:T(8,128)(2,1)S(1)}, bf16[128,256]{1,0:T(8,128)(2,1)S(1)}, u32[]{:S(2)}, u32[]{:S(2)}) collective-permute-start(bf16[128,256]{1,0:T(8,128)(2,1)S(1)} %slice_bitcast_fusion.refs_0_), channel_id=1, source_target_pairs={{0,7},{1,0},{2,1},{3,2},{4,3},{5,4},{6,5},{7,6},{8,15},{9,8},{10,9... | collective-permute-start | bytes 196616 | tf_op jit(solution)/shard_map/ppermute | solution.py:70
  43.2 8.0 %collective-permute-start.4 = (bf16[128,256]{1,0:T(8,128)(2,1)S(1)}, bf16[128,256]{1,0:T(8,128)(2,1)S(1)}, u32[]{:S(2)}, u32[]{:S(2)}) collective-permute-start(bf16[128,256]{1,0:T(8,128)(2,1)S(1)} %collective-permute-done.3.refs_7_), channel_id=1, source_target_pairs={{0,1},{1,2},{2,3},{3,4},{4,5},{5,6},{6,7},{7,0},{8,9},{9,10},{10,1... | collective-permute-start | bytes 196616 | tf_op jit(solution)/shard_map/ppermute | solution.py:68
  43.2 16.4 %collective-permute-start.7 = (bf16[272,512]{1,0:T(8,128)(2,1)}, bf16[272,512]{1,0:T(8,128)(2,1)S(1)}, u32[]{:S(2)}, u32[]{:S(2)}) collective-permute-start(bf16[272,512]{1,0:T(8,128)(2,1)} %pack.3.refs_0_), channel_id=1, source_target_pairs={{0,7},{1,0},{2,1},{3,2},{4,3},{5,4},{6,5},{7,6},{8,15},{9,8},{10,9... | collective-permute-start | bytes 835592 | tf_op jit(solution)/shard_map/ppermute | solution.py:70
  45.9 16.4 %collective-permute-start.11 = (bf16[272,512]{1,0:T(8,128)(2,1)S(1)}, bf16[272,512]{1,0:T(8,128)(2,1)S(1)}, u32[]{:S(2)}, u32[]{:S(2)}) collective-permute-start(bf16[272,512]{1,0:T(8,128)(2,1)S(1)} %collective-permute-done.10.refs_7_), channel_id=1, source_target_pairs={{0,1},{1,2},{2,3},{3,4},{4,5},{5,6},{6,7},{7,0},{8,9},{9,10},{10,1... | collective-permute-start | bytes 835592 | tf_op jit(solution)/shard_map/ppermute | solution.py:68
  49.4 8.4 %collective-permute-start.1 = (bf16[128,256]{1,0:T(8,128)(2,1)S(1)}, bf16[128,256]{1,0:T(8,128)(2,1)S(1)}, u32[]{:S(2)}, u32[]{:S(2)}) collective-permute-start(bf16[128,256]{1,0:T(8,128)(2,1)S(1)} %collective-permute-done.refs_1_), channel_id=1, source_target_pairs={{0,7},{1,0},{2,1},{3,2},{4,3},{5,4},{6,5},{7,6},{8,15},{9,8},{10,9... | collective-permute-start | bytes 196616 | tf_op jit(solution)/shard_map/ppermute | solution.py:70
  51.2 8.4 %collective-permute-start.5 = (bf16[128,256]{1,0:T(8,128)(2,1)S(1)}, bf16[128,256]{1,0:T(8,128)(2,1)S(1)}, u32[]{:S(2)}, u32[]{:S(2)}) collective-permute-start(bf16[128,256]{1,0:T(8,128)(2,1)S(1)} %collective-permute-done.4.refs_6_), channel_id=1, source_target_pairs={{0,1},{1,2},{2,3},{3,4},{4,5},{5,6},{6,7},{7,0},{8,9},{9,10},{10,1... | collective-permute-start | bytes 196616 | tf_op jit(solution)/shard_map/ppermute | solution.py:68
  57.8 4.6 %collective-permute-start.2 = (bf16[128,256]{1,0:T(8,128)(2,1)S(1)}, bf16[128,256]{1,0:T(8,128)(2,1)S(1)}, u32[]{:S(2)}, u32[]{:S(2)}) collective-permute-start(bf16[128,256]{1,0:T(8,128)(2,1)S(1)} %collective-permute-done.1.refs_2_), channel_id=1, source_target_pairs={{0,7},{1,0},{2,1},{3,2},{4,3},{5,4},{6,5},{7,6},{8,15},{9,8},{10,9... | collective-permute-start | bytes 196616 | tf_op jit(solution)/shard_map/ppermute | solution.py:70
  59.6 4.3 %collective-permute-start.6 = (bf16[128,256]{1,0:T(8,128)(2,1)S(1)}, bf16[128,256]{1,0:T(8,128)(2,1)S(1)}, u32[]{:S(2)}, u32[]{:S(2)}) collective-permute-start(bf16[128,256]{1,0:T(8,128)(2,1)S(1)} %collective-permute-done.5.refs_5_), channel_id=1, source_target_pairs={{0,1},{1,2},{2,3},{3,4},{4,5},{5,6},{6,7},{7,0},{8,9},{9,10},{10,1... | collective-permute-start | bytes 196616 | tf_op jit(solution)/shard_map/ppermute | solution.py:68
  59.6 18.1 %collective-permute-start.8 = (bf16[272,512]{1,0:T(8,128)(2,1)S(1)}, bf16[272,512]{1,0:T(8,128)(2,1)S(1)}, u32[]{:S(2)}, u32[]{:S(2)}) collective-permute-start(bf16[272,512]{1,0:T(8,128)(2,1)S(1)} %collective-permute-done.7.refs_1_), channel_id=1, source_target_pairs={{0,7},{1,0},{2,1},{3,2},{4,3},{5,4},{6,5},{7,6},{8,15},{9,8},{10,9... | collective-permute-start | bytes 835592 | tf_op jit(solution)/shard_map/ppermute | solution.py:70
  62.3 16.3 %collective-permute-start.12 = (bf16[272,512]{1,0:T(8,128)(2,1)S(1)}, bf16[272,512]{1,0:T(8,128)(2,1)S(1)}, u32[]{:S(2)}, u32[]{:S(2)}) collective-permute-start(bf16[272,512]{1,0:T(8,128)(2,1)S(1)} %collective-permute-done.11.refs_6_), channel_id=1, source_target_pairs={{0,1},{1,2},{2,3},{3,4},{4,5},{5,6},{6,7},{7,0},{8,9},{9,10},{10,1... | collective-permute-start | bytes 835592 | tf_op jit(solution)/shard_map/ppermute | solution.py:68
  68.7 17.9 %all-to-all-start.2 = ((f16[16,32,128]{2,1,0:T(8,128)(2,1)}), f16[16,32,128]{2,1,0:T(8,128)(2,1)S(1)}, u32[]{:S(2)}, u32[]{:S(2)}) async-start(f16[16,32,128]{2,1,0:T(8,128)(2,1)} %convert_element_type.24), calls=%async_computation.2 | async-start | bytes 262144 | tf_op jit(solution)/shard_map/all_to_all | solution.py:27
  77.7 13.3 %collective-permute-start.9 = (bf16[272,512]{1,0:T(8,128)(2,1)S(1)}, bf16[272,512]{1,0:T(8,128)(2,1)S(1)}, u32[]{:S(2)}, u32[]{:S(2)}) collective-permute-start(bf16[272,512]{1,0:T(8,128)(2,1)S(1)} %collective-permute-done.8.refs_2_), channel_id=1, source_target_pairs={{0,7},{1,0},{2,1},{3,2},{4,3},{5,4},{6,5},{7,6},{8,15},{9,8},{10,9... | collective-permute-start | bytes 835592 | tf_op jit(solution)/shard_map/ppermute | solution.py:70
  78.6 12.4 %collective-permute-start.13 = (bf16[272,512]{1,0:T(8,128)(2,1)S(1)}, bf16[272,512]{1,0:T(8,128)(2,1)S(1)}, u32[]{:S(2)}, u32[]{:S(2)}) collective-permute-start(bf16[272,512]{1,0:T(8,128)(2,1)S(1)} %collective-permute-done.12.refs_5_), channel_id=1, source_target_pairs={{0,1},{1,2},{2,3},{3,4},{4,5},{5,6},{6,7},{7,0},{8,9},{9,10},{10,1... | collective-permute-start | bytes 835592 | tf_op jit(solution)/shard_map/ppermute | solution.py:68
  87.3 12.4 %all-to-all-start.3 = ((bf16[16,32,128]{2,1,0:T(8,128)(2,1)}), bf16[16,32,128]{2,1,0:T(8,128)(2,1)S(1)}, u32[]{:S(2)}, u32[]{:S(2)}) async-start(bf16[16,32,128]{2,1,0:T(8,128)(2,1)} %next.1), calls=%async_computation.3 | async-start | bytes 262144 | tf_op jit(solution)/shard_map/all_to_all | solution.py:27
  99.7 20.0 %copy-start.4 = (bf16[2,128,256]{2,1,0:T(8,128)(2,1)S(1)}, bf16[2,128,256]{2,1,0:T(8,128)(2,1)}, u32[]{:S(2)}) copy-start(bf16[2,128,256]{2,1,0:T(8,128)(2,1)} %w_ref.1) | copy-start | bytes 393220

commit v4 on v3

--- a/solution.py
+++ b/solution.py
@@ -6,6 +6,7 @@
 from jax.experimental import pallas as pl
 from jax.experimental.pallas import tpu as pltpu
 from jax.sharding import PartitionSpec as P
+
 
 D = 2048
 LENGTH_MEAN = 512
@@ -16,7 +17,8 @@
 PARAMS = pltpu.CompilerParams(vmem_limit_bytes=16 << 20)
 WIDE_PARAMS = pltpu.CompilerParams(vmem_limit_bytes=51 << 20)
 SECOND_PARAMS = pltpu.CompilerParams(vmem_limit_bytes=49 << 20)
-PACK_PARAMS = pltpu.CompilerParams(vmem_limit_bytes=54900 << 10)
+PREP_PARAMS = pltpu.CompilerParams(vmem_limit_bytes=54900 << 10)
+PACK_PARAMS = pltpu.CompilerParams(vmem_limit_bytes=55300 << 10)
 VMEM = pl.BlockSpec(memory_space=pltpu.VMEM)
 HBM = pl.BlockSpec(memory_space=pltpu.HBM)
 
@@ -59,15 +61,45 @@
     )(gain, *weights)
 
 
-def around(shard, axis):
+def prep_kernel(gain_ref, *refs):
+    weights, row_ref, firsts, sems = refs[:4], refs[4], refs[5:9], refs[9]
+    copies = [pltpu.make_async_copy(w_ref.at[0], out, sems.at[n]) for n, (w_ref, out) in enumerate(zip(weights, firsts))]
+    for copy in copies:
+        copy.start()
+    row_ref[...] = gain_ref[0:1, :].astype(jnp.float32)
+    for copy in copies:
+        copy.wait()
+
+
+def prep(gain, weights):
+    return pl.pallas_call(
+        prep_kernel,
+        in_specs=[VMEM] + [HBM] * len(weights),
+        out_specs=[VMEM] * (1 + len(weights)),
+        out_shape=[jax.ShapeDtypeStruct((1, gain.shape[1]), jnp.float32)]
+        + [jax.ShapeDtypeStruct(w.shape[1:], w.dtype) for w in weights],
+        scratch_shapes=[pltpu.SemaphoreType.DMA((len(weights),))],
+        compiler_params=PREP_PARAMS,
+        name="prep",
+    )(gain, *weights)
+
+
+def after(x, y):
+    return lax.optimization_barrier((x, y))[0]
+
+
+def around(shard, axis, gates):
     size = lax.axis_size(axis)
     onward = [(n, (n + 1) % size) for n in range(size)]
     back = [(n, (n - 1) % size) for n in range(size)]
     held = {0: shard}
     for step in range(1, size // 2 + 1):
-        held[size - step] = lax.ppermute(held[(size - step + 1) % size], axis, onward)
+        left, right = held[size - step + 1 if step > 1 else 0], held[step - 1]
+        if step in gates:
+            left, right = after(left, gates[step]), after(right, gates[step])
+        held[size - step] = lax.ppermute(left, axis, onward)
         if step < size // 2:
-            held[step] = lax.ppermute(held[step - 1], axis, back)
+            held[step] = lax.ppermute(right, axis, back)
     return [held[n] for n in range(size)]
 
 
@@ -84,7 +116,7 @@
     return jnp.where(total < 0.0, -root, root)
 
 
-def project_kernel(share, x_ref, w_ref, out_ref):
+def project_kernel(share, x_ref, gain_ref, wq_ref, wf_ref, wi_ref, wg_ref, out_ref):
     owners, size = out_ref.shape[0], out_ref.shape[-1]
     rows = out_ref.shape[1] // 5
     held = x_ref[...].reshape(owners * rows, x_ref.shape[-1])
@@ -93,11 +125,10 @@
     power = jnp.ceil(0.5 * jnp.log2(jnp.maximum(squares, FLOOR)))
     down = jnp.exp2(-power)
     factor = down * 2.0**13
-    features = x.shape[1]
-    gained = (x * w_ref[features : features + 1, :features].astype(jnp.float32)).astype(jnp.bfloat16)
-    partial = factor * jnp.dot(gained, w_ref[:features, :], preferred_element_type=jnp.float32)
-    for n in range(4):
-        out_ref[:, n * rows : (n + 1) * rows, :] = partial[:, n * size : (n + 1) * size].reshape(owners, rows, size)
+    gained = (x * gain_ref[...]).astype(jnp.bfloat16)
+    for n, w_ref in enumerate((wq_ref, wf_ref, wi_ref, wg_ref)):
+        partial = factor * jnp.dot(gained, w_ref[...], preferred_element_type=jnp.float32)
+        out_ref[:, n * rows : (n + 1) * rows, :] = partial.reshape(owners, rows, size)
     mantissa = squares * down * down
     high = mantissa.astype(jnp.bfloat16).astype(jnp.float32)
     lane = lax.broadcasted_iota(jnp.int32, (owners * rows, size), 1)
@@ -107,15 +138,15 @@
     out_ref[:, 4 * rows :, :] = (table + kept).reshape(owners, rows, size)
 
 
-def project(whole, weight, owners):
+def project(whole, gain, weights, owners):
     rows = whole.shape[0] * whole.shape[1] // owners
     share = whole.shape[2] // lax.axis_size("tp")
     return pl.pallas_call(
         functools.partial(project_kernel, share),
-        out_shape=jax.ShapeDtypeStruct((owners, 5 * rows, weight.shape[1] // 4), jnp.float32),
+        out_shape=jax.ShapeDtypeStruct((owners, 5 * rows, weights[0].shape[1]), jnp.float32),
         compiler_params=PARAMS,
         name="project",
-    )(whole, weight)
+    )(whole, gain, *weights)
 
 
 def moves(block, state_ref, new_ref, prior_s, new_s, in_sems, out_sems):
@@ -283,7 +314,7 @@
     out_ref[...] = decoded(parts_ref)
 
 
-def shards(
+def layers(
     tokens,
     state,
     lengths,
@@ -300,22 +331,25 @@
     tp, dp = lax.axis_size("tp"), lax.axis_size("dp")
     whole = exchange(jnp.broadcast_to(tokens, (tp, *tokens.shape)), "tp")
     weights = (w_query, w_forget, w_input, w_gate)
-    back = around(w_out[0], "dp")
-    weight = pack(0, norm_gain, weights)
-    held = around(pack(1, norm_gain, weights), "dp")
+    gain, *firsts = prep(norm_gain, weights)
+    back = around(w_out[0], "dp", {})
+    whole = after(whole, (back[3], back[dp - 3]))
     log_len = jnp.log(lengths.astype(jnp.float32) / LENGTH_MEAN)
     shift = pace[:, None, :] * log_len[None, :, None]
 
-    parts = exchange_products(project(whole, weight, dp), "dp")
-    target, parts = first(parts, shift, bound_logit, head_gain, back, state)
-    parts = exchange_products(parts, "tp")
+    message = project(whole, gain, firsts, dp).astype(jnp.float16)
+    parts = exchange(message, "dp").astype(jnp.float32)
+    target, sums = first(parts, shift, bound_logit, head_gain, back, state)
+    held = around(pack(1, after(norm_gain, message), weights), "dp", {2: sums})
+    parts = exchange_products(sums, "tp")
     copies = pl.pallas_call(
         next_kernel,
         out_shape=jax.ShapeDtypeStruct(parts.shape, jnp.bfloat16),
         compiler_params=PARAMS,
         name="next",
     )(parts)
-    target, normed = second(exchange(copies, "tp"), shift, bound_logit, head_gain, held, state, target)
+    joined = exchange(copies, "tp")
+    target, normed = second(joined, shift, bound_logit, head_gain, held, state, target)
     parts = exchange_products(branch_parts(exchange(normed, "dp"), w_out, tp), "tp")
     result = pl.pallas_call(
         final_kernel,
@@ -342,4 +376,4 @@
         P(),
     )
     out_specs = (P(("grp", "tp"), "dp"), P(None, ("grp", "dp"), "tp", None, None))
-    return jax.shard_map(shards, mesh=mesh, in_specs=in_specs, out_specs=out_specs, check_vma=False)
+    return jax.shard_map(layers, mesh=mesh, in_specs=in_specs, out_specs=out_specs, check_vma=False)

time: 134 us -> 138 us (1.030)
  blocking collectives: 28 us -> 38.9 us
  waiting for transfers between devices: 30.2 us -> 21.5 us
  starting transfers between devices: 53.1 us -> 58.4 us
  local copies, waits for them, and re-layouts: 5.68 us -> 2.93 us
    all_to_all x2 -> x3, blocking collectives: 28 us -> 38.9 us  [exchange(): return lax.all_to_all(x, axis, split_axis=0, concat_axis=0, tiled=True)]
    all_to_all x4 -> x3, waiting for transfers between devices: 18.5 us -> 9.18 us  [exchange(): return lax.all_to_all(x, axis, split_axis=0, concat_axis=0, tiled=True)]
    ppermute x14, starting transfers between devices: 13.1 us -> 18.2 us  [the longest x6 14.7 us: around(): held[step] = lax.ppermute(right, axis, back)]
    unnamed x20 -> x14, local copies, waits for them, and re-layouts: 3.46 us -> 0.71 us
    pallas_call x2 -> x1, Pallas kernels: 3.27 us -> 2.36 us  [pack(): pl.pallas_call(functools.partial(pack_kernel, block), in_specs=[VMEM] + [...]
    all_to_all x4 -> x3, starting transfers between devices: 40.1 us -> 40.2 us  [exchange(): return lax.all_to_all(x, axis, split_axis=0, concat_axis=0, tiled=True)]
  transfers between devices with their start and end apart: 18 -> 17, of which waited for: 6 -> 6; matrix products, arithmetic and copies ran while one was open for 2% -> 1% of each run, Pallas kernels for 6% -> 5%
where the time goes in v4:
time: 138 us; the launch traced here: 137 us
  starting transfers between devices  58.4 us (42%)
  blocking collectives  38.9 us (28%)
  waiting for transfers between devices  21.5 us (16%)
  Pallas kernels  12.8 us (9%)
  local copies, waits for them, and re-layouts  2.93 us (2%)
  other arithmetic  1.62 us (1%)
    all_to_all x3, starting transfers between devices, exchange(): return lax.all_to_all(x, axis, split_axis=0, concat_axis=0, tiled=True)  40.2 us
    all_to_all x3, blocking collectives, exchange(): return lax.all_to_all(x, axis, split_axis=0, concat_axis=0, tiled=True)  38.9 us
    ppermute x6, starting transfers between devices, around(): held[step] = lax.ppermute(right, axis, back)  14.7 us
    ppermute x8, waiting for transfers between devices, around(): held[size - step] = lax.ppermute(left, axis, onward)  12.4 us
    all_to_all x3, waiting for transfers between devices, exchange(): return lax.all_to_all(x, axis, split_axis=0, concat_axis=0, tiled=True)  9.18 us
    pallas_call x1, Pallas kernels, second(): pl.pallas_call(functools.partial(second_kernel, rows // lax.axis_size('tp...  4.15 us
    pallas_call x1, Pallas kernels, first(): pl.pallas_call(functools.partial(first_kernel, shards[0].shape[1] // tp),...  4.06 us
    ppermute x8, starting transfers between devices, around(): held[size - step] = lax.ppermute(left, axis, onward)  3.45 us
  transfers between devices with their start and end apart: 17, of which 6 were waited for; matrix products, arithmetic and copies ran while one was open for 1% of the time, Pallas kernels for 5%

profile of v4, /device:TPU:513, one launch (start us, length us, event | category | flops | bytes accessed | tf_op | source)
XLA Modules:
  0.0 137.0 jit_solution(6378580550076923920)
XLA Ops:
  0.7 1.4 %broadcast_in_dim.2 = bf16[16,16,256]{2,1,0:T(8,128)(2,1)} broadcast(bf16[16,256]{1,0:T(8,128)(2,1)} %param.12), dimensions={1,2} | broadcast | bytes 139264 | tf_op jit(solution)/shard_map/broadcast_in_dim | solution.py:332
  2.1 23.7 %all-to-all-start = ((bf16[16,16,256]{2,1,0:T(8,128)(2,1)}), bf16[16,16,256]{2,1,0:T(8,128)(2,1)S(1)}, u32[]{:S(2)}, u32[]{:S(2)}) async-start(bf16[16,16,256]{2,1,0:T(8,128)(2,1)} %broadcast_in_dim.2), calls=%async_computation | async-start | bytes 262144 | tf_op jit(solution)/shard_map/all_to_all | solution.py:29
  25.8 0.8 slice_bitcast_fusion.refs_0_
  26.6 0.0 collective-permute-start.3
  26.6 2.7 %collective-permute-start = (bf16[128,256]{1,0:T(8,128)(2,1)S(1)}, bf16[128,256]{1,0:T(8,128)(2,1)S(1)}, u32[]{:S(2)}, u32[]{:S(2)}) collective-permute-start(bf16[128,256]{1,0:T(8,128)(2,1)S(1)} %slice_bitcast_fusion.refs_0_), channel_id=1, source_target_pairs={{0,7},{1,0},{2,1},{3,2},{4,3},{5,4},{6,5},{7,6},{8,15},{9,8},{10,9... | collective-permute-start | bytes 196616 | tf_op jit(solution)/shard_map/ppermute | solution.py:102
  29.3 1.9 %collective-permute-done.3.refs_7_ = bf16[128,256]{1,0:T(8,128)(2,1)S(1)} collective-permute-done((bf16[128,256]{1,0:T(8,128)(2,1)S(1)}, bf16[128,256]{1,0:T(8,128)(2,1)S(1)}, u32[]{:S(2)}, u32[]{:S(2)}) %collective-permute-start.3) | collective-permute-done | bytes 65568 | tf_op jit(solution)/shard_map/ppermute | solution.py:100
  31.2 0.0 collective-permute-start.4
  31.3 0.0 collective-permute-done.refs_1_
  31.3 2.7 %collective-permute-start.1 = (bf16[128,256]{1,0:T(8,128)(2,1)S(1)}, bf16[128,256]{1,0:T(8,128)(2,1)S(1)}, u32[]{:S(2)}, u32[]{:S(2)}) collective-permute-start(bf16[128,256]{1,0:T(8,128)(2,1)S(1)} %collective-permute-done.refs_1_), channel_id=1, source_target_pairs={{0,7},{1,0},{2,1},{3,2},{4,3},{5,4},{6,5},{7,6},{8,15},{9,8},{10,9... | collective-permute-start | bytes 196616 | tf_op jit(solution)/shard_map/ppermute | solution.py:102
  33.9 1.6 %collective-permute-done.4.refs_6_ = bf16[128,256]{1,0:T(8,128)(2,1)S(1)} collective-permute-done((bf16[128,256]{1,0:T(8,128)(2,1)S(1)}, bf16[128,256]{1,0:T(8,128)(2,1)S(1)}, u32[]{:S(2)}, u32[]{:S(2)}) %collective-permute-start.4) | collective-permute-done | bytes 65568 | tf_op jit(solution)/shard_map/ppermute | solution.py:100
  35.6 0.0 collective-permute-start.5
  35.6 0.0 collective-permute-done.1.refs_2_
  35.6 2.7 %collective-permute-start.2 = (bf16[128,256]{1,0:T(8,128)(2,1)S(1)}, bf16[128,256]{1,0:T(8,128)(2,1)S(1)}, u32[]{:S(2)}, u32[]{:S(2)}) collective-permute-start(bf16[128,256]{1,0:T(8,128)(2,1)S(1)} %collective-permute-done.1.refs_2_), channel_id=1, source_target_pairs={{0,7},{1,0},{2,1},{3,2},{4,3},{5,4},{6,5},{7,6},{8,15},{9,8},{10,9... | collective-permute-start | bytes 196616 | tf_op jit(solution)/shard_map/ppermute | solution.py:102
  38.3 0.7 copy-done.2
  38.9 1.0 prep.1
  39.9 0.0 collective-permute-done.5.refs_5_
  39.9 0.0 collective-permute-done.2.refs_3_
  39.9 0.0 all-to-all-done.x_ref
  39.9 0.3 project.1
  40.3 0.8 convert_element_type.21
  41.0 3.9 %all-to-all-start.1 = ((f16[8,160,128]{2,1,0:T(8,128)(2,1)}), f16[8,160,128]{2,1,0:T(8,128)(2,1)S(1)}, u32[]{:S(2)}, u32[]{:S(2)}) async-start(f16[8,160,128]{2,1,0:T(8,128)(2,1)} %convert_element_type.21), calls=%async_computation.1 | async-start | bytes 655360 | tf_op jit(solution)/shard_map/all_to_all | solution.py:29
  45.0 2.4 %pack.1.refs_0_ = bf16[272,512]{1,0:T(8,128)(2,1)} custom-call(bf16[2,256]{1,0:T(2,128)(2,1)} %gain_ref.2, bf16[2,256,128]{2,1,0:T(8,128)(2,1)} %wq_ref.1, bf16[2,256,128]{2,1,0:T(8,128)(2,1)} %wf_ref.1, bf16[2,256,128]{2,1,0:T(8,128)(2,1)} %wi_ref.1, bf16[2,256,128]{2,1,0:T(8,128)(2,1)} %wg_ref.1), custom_call_target="tpu_custom_call" | custom-call | tf_op jit(solution)/shard_map/pack/pallas_call | solution.py:53
  47.4 1.6 %collective-permute-start.10 = (bf16[272,512]{1,0:T(8,128)(2,1)}, bf16[272,512]{1,0:T(8,128)(2,1)S(1)}, u32[]{:S(2)}, u32[]{:S(2)}) collective-permute-start(bf16[272,512]{1,0:T(8,128)(2,1)} %pack.1.refs_0_), channel_id=1, source_target_pairs={{0,1},{1,2},{2,3},{3,4},{4,5},{5,6},{6,7},{7,0},{8,9},{9,10},{10,1... | collective-permute-start | bytes 835592 | tf_op jit(solution)/shard_map/ppermute | solution.py:100
  48.9 1.2 collective-permute-start.6
  50.1 0.1 broadcast_multiply_fusion.shift_ref
  50.2 1.5 %collective-permute-start.7 = (bf16[272,512]{1,0:T(8,128)(2,1)}, bf16[272,512]{1,0:T(8,128)(2,1)S(1)}, u32[]{:S(2)}, u32[]{:S(2)}) collective-permute-start(bf16[272,512]{1,0:T(8,128)(2,1)} %pack.1.refs_0_), channel_id=1, source_target_pairs={{0,7},{1,0},{2,1},{3,2},{4,3},{5,4},{6,5},{7,6},{8,15},{9,8},{10,9... | collective-permute-start | bytes 835592 | tf_op jit(solution)/shard_map/ppermute | solution.py:102
  51.7 3.4 %all-to-all-done.1 = f16[8,160,128]{2,1,0:T(8,128)(2,1)S(1)} async-done(((f16[8,160,128]{2,1,0:T(8,128)(2,1)}), f16[8,160,128]{2,1,0:T(8,128)(2,1)S(1)}, u32[]{:S(2)}, u32[]{:S(2)}) %all-to-all-start.1) | async-done | bytes 327712 | tf_op jit(solution)/shard_map/all_to_all | solution.py:29
  55.2 4.8 %collective-permute-done.6.refs_4_ = bf16[128,256]{1,0:T(8,128)(2,1)S(1)} collective-permute-done((bf16[128,256]{1,0:T(8,128)(2,1)S(1)}, bf16[128,256]{1,0:T(8,128)(2,1)S(1)}, u32[]{:S(2)}, u32[]{:S(2)}) %collective-permute-start.6) | collective-permute-done | bytes 65568 | tf_op jit(solution)/shard_map/ppermute | solution.py:100
  60.0 4.1 %first.1 = (f32[2,32,1,128,128]{4,3,2,1,0:T(8,128)}, f32[16,32,128]{2,1,0:T(8,128)S(1)}) custom-call(f32[8,160,128]{2,1,0:T(8,128)S(1)} %convert_element_type.22.parts_ref, f32[2,32,128]{2,1,0:T(8,128)S(1)} %broadcast_multiply_fusion.shift_ref, f32[2,128]{1,0:T(2,128)S(1)} %copy-done.3, f32[2,128]{1,0:T(2,128)S(1)} %copy-done.4, ...), custom_call_target="tpu_custom_call" | custom-call | tf_op jit(solution)/shard_map/first/pallas_call | solution.py:223
  64.1 0.7 collective-permute-start.11
  64.7 0.0 collective-permute-done.7.refs_1_
  64.7 2.1 %collective-permute-start.8 = (bf16[272,512]{1,0:T(8,128)(2,1)S(1)}, bf16[272,512]{1,0:T(8,128)(2,1)S(1)}, u32[]{:S(2)}, u32[]{:S(2)}) collective-permute-start(bf16[272,512]{1,0:T(8,128)(2,1)S(1)} %collective-permute-done.7.refs_1_), channel_id=1, source_target_pairs={{0,7},{1,0},{2,1},{3,2},{4,3},{5,4},{6,5},{7,6},{8,15},{9,8},{10,9... | collective-permute-start | bytes 835592 | tf_op jit(solution)/shard_map/ppermute | solution.py:102
  66.9 3.9 %collective-permute-done.11.refs_6_ = bf16[272,512]{1,0:T(8,128)(2,1)S(1)} collective-permute-done((bf16[272,512]{1,0:T(8,128)(2,1)S(1)}, bf16[272,512]{1,0:T(8,128)(2,1)S(1)}, u32[]{:S(2)}, u32[]{:S(2)}) %collective-permute-start.11) | collective-permute-done | bytes 278560 | tf_op jit(solution)/shard_map/ppermute | solution.py:100
  70.8 0.0 collective-permute-start.12
  70.8 0.7 convert_element_type.24
  71.5 12.5 %all-to-all-start.2 = ((f16[16,32,128]{2,1,0:T(8,128)(2,1)}), f16[16,32,128]{2,1,0:T(8,128)(2,1)S(1)}, u32[]{:S(2)}, u32[]{:S(2)}) async-start(f16[16,32,128]{2,1,0:T(8,128)(2,1)} %convert_element_type.24), calls=%async_computation.2 | async-start | bytes 262144 | tf_op jit(solution)/shard_map/all_to_all | solution.py:29
  84.0 3.1 %collective-permute-start.9 = (bf16[272,512]{1,0:T(8,128)(2,1)S(1)}, bf16[272,512]{1,0:T(8,128)(2,1)S(1)}, u32[]{:S(2)}, u32[]{:S(2)}) collective-permute-start(bf16[272,512]{1,0:T(8,128)(2,1)S(1)} %collective-permute-done.8.refs_2_), channel_id=1, source_target_pairs={{0,7},{1,0},{2,1},{3,2},{4,3},{5,4},{6,5},{7,6},{8,15},{9,8},{10,9... | collective-permute-start | bytes 835592 | tf_op jit(solution)/shard_map/ppermute | solution.py:102
  87.0 0.0 collective-permute-done.12.refs_5_
  87.0 5.8 %all-to-all-done.2 = f16[16,32,128]{2,1,0:T(8,128)(2,1)S(1)} async-done(((f16[16,32,128]{2,1,0:T(8,128)(2,1)}), f16[16,32,128]{2,1,0:T(8,128)(2,1)S(1)}, u32[]{:S(2)}, u32[]{:S(2)}) %all-to-all-start.2) | async-done | bytes 131104 | tf_op jit(solution)/shard_map/all_to_all | solution.py:29
  92.9 11.6 %all_to_all.30.x_ref = bf16[16,32,128]{2,1,0:T(8,128)(2,1)S(1)} all-to-all(bf16[16,32,128]{2,1,0:T(8,128)(2,1)S(1)} %next.1), channel_id=1, replica_groups=mesh['grp'=2,'tp'=16,'dp'=8] {'tp'}, dimensions={0} | all-to-all | bytes 262144 | tf_op jit(solution)/shard_map/all_to_all | solution.py:29
  104.5 0.0 collective-permute-done.9.refs_3_
  104.5 0.0 collective-permute-done.13.refs_4_
  104.5 0.0 copy-start.1
  104.5 4.2 %second.1 = (f32[2,32,1,128,128]{4,3,2,1,0:T(8,128)}, bf16[8,64,128]{2,1,0:T(8,128)(2,1)S(1)}) custom-call(bf16[16,32,128]{2,1,0:T(8,128)(2,1)S(1)} %all_to_all.30.x_ref, f32[2,32,128]{2,1,0:T(8,128)S(1)} %broadcast_multiply_fusion.shift_ref, f32[2,128]{1,0:T(2,128)S(1)} %copy-done.3, f32[2,128]{1,0:T(2,128)S(1)} %copy-done.4, ...), custom_call_target="tpu_custom_call", output_to_operand_aliasing={{0}: (13, {})} | custom-call | tf_op jit(solution)/shard_map/second/pallas_call | solution.py:277
  108.7 14.3 %all_to_all.31.normed_ref = bf16[8,64,128]{2,1,0:T(8,128)(2,1)S(1)} all-to-all(bf16[8,64,128]{2,1,0:T(8,128)(2,1)S(1)} %get-tuple-element.26), channel_id=1, replica_groups=mesh['grp'=2,'tp'=16,'dp'=8] {'dp'}, dimensions={0} | all-to-all | bytes 262144 | tf_op jit(solution)/shard_map/all_to_all | solution.py:29
  123.0 0.3 branch.1
  123.3 13.0 %all_to_all.32 = f16[16,16,256]{2,1,0:T(8,128)(2,1)S(1)} all-to-all(f16[16,16,256]{2,1,0:T(8,128)(2,1)S(1)} %convert_element_type.26), channel_id=1, replica_groups=mesh['grp'=2,'tp'=16,'dp'=8] {'tp'}, dimensions={0} | all-to-all | bytes 262144 | tf_op jit(solution)/shard_map/all_to_all | solution.py:29
  136.4 0.6 final.1
  (21 shorter events, 0.2 us)
Async XLA Ops:
  0.6 48.3 %copy-start.6 = (s32[32]{0:T(128)S(1)}, s32[32]{0:T(128)}, u32[]{:S(2)}) copy-start(s32[32]{0:T(128)} %param.14) | copy-start | bytes 388
  0.6 49.5 %copy-start.5 = (f32[2,128]{1,0:T(2,128)S(1)}, f32[2,128]{1,0:T(2,128)}, u32[]{:S(2)}) copy-start(f32[2,128]{1,0:T(2,128)} %param.22) | copy-start | bytes 3076
  0.7 59.3 %copy-start.4 = (f32[2,128]{1,0:T(2,128)S(1)}, f32[2,128]{1,0:T(2,128)}, u32[]{:S(2)}) copy-start(f32[2,128]{1,0:T(2,128)} %head_ref.3) | copy-start | bytes 3076
  0.7 59.3 %copy-start.3 = (f32[2,128]{1,0:T(2,128)S(1)}, f32[2,128]{1,0:T(2,128)}, u32[]{:S(2)}) copy-start(f32[2,128]{1,0:T(2,128)} %bound_ref.3) | copy-start | bytes 3076
  2.1 37.9 %all-to-all-start = ((bf16[16,16,256]{2,1,0:T(8,128)(2,1)}), bf16[16,16,256]{2,1,0:T(8,128)(2,1)S(1)}, u32[]{:S(2)}, u32[]{:S(2)}) async-start(bf16[16,16,256]{2,1,0:T(8,128)(2,1)} %broadcast_in_dim.2), calls=%async_computation | async-start | bytes 262144 | tf_op jit(solution)/shard_map/all_to_all | solution.py:29
  26.6 4.6 %collective-permute-start.3 = (bf16[128,256]{1,0:T(8,128)(2,1)S(1)}, bf16[128,256]{1,0:T(8,128)(2,1)S(1)}, u32[]{:S(2)}, u32[]{:S(2)}) collective-permute-start(bf16[128,256]{1,0:T(8,128)(2,1)S(1)} %slice_bitcast_fusion.refs_0_), channel_id=1, source_target_pairs={{0,1},{1,2},{2,3},{3,4},{4,5},{5,6},{6,7},{7,0},{8,9},{9,10},{10,1... | collective-permute-start | bytes 196616 | tf_op jit(solution)/shard_map/ppermute | solution.py:100
  26.6 4.6 %collective-permute-start = (bf16[128,256]{1,0:T(8,128)(2,1)S(1)}, bf16[128,256]{1,0:T(8,128)(2,1)S(1)}, u32[]{:S(2)}, u32[]{:S(2)}) collective-permute-start(bf16[128,256]{1,0:T(8,128)(2,1)S(1)} %slice_bitcast_fusion.refs_0_), channel_id=1, source_target_pairs={{0,7},{1,0},{2,1},{3,2},{4,3},{5,4},{6,5},{7,6},{8,15},{9,8},{10,9... | collective-permute-start | bytes 196616 | tf_op jit(solution)/shard_map/ppermute | solution.py:102
  31.2 4.3 %collective-permute-start.4 = (bf16[128,256]{1,0:T(8,128)(2,1)S(1)}, bf16[128,256]{1,0:T(8,128)(2,1)S(1)}, u32[]{:S(2)}, u32[]{:S(2)}) collective-permute-start(bf16[128,256]{1,0:T(8,128)(2,1)S(1)} %collective-permute-done.3.refs_7_), channel_id=1, source_target_pairs={{0,1},{1,2},{2,3},{3,4},{4,5},{5,6},{6,7},{7,0},{8,9},{9,10},{10,1... | collective-permute-start | bytes 196616 | tf_op jit(solution)/shard_map/ppermute | solution.py:100
  31.3 4.3 %collective-permute-start.1 = (bf16[128,256]{1,0:T(8,128)(2,1)S(1)}, bf16[128,256]{1,0:T(8,128)(2,1)S(1)}, u32[]{:S(2)}, u32[]{:S(2)}) collective-permute-start(bf16[128,256]{1,0:T(8,128)(2,1)S(1)} %collective-permute-done.refs_1_), channel_id=1, source_target_pairs={{0,7},{1,0},{2,1},{3,2},{4,3},{5,4},{6,5},{7,6},{8,15},{9,8},{10,9... | collective-permute-start | bytes 196616 | tf_op jit(solution)/shard_map/ppermute | solution.py:102
  35.6 4.3 %collective-permute-start.5 = (bf16[128,256]{1,0:T(8,128)(2,1)S(1)}, bf16[128,256]{1,0:T(8,128)(2,1)S(1)}, u32[]{:S(2)}, u32[]{:S(2)}) collective-permute-start(bf16[128,256]{1,0:T(8,128)(2,1)S(1)} %collective-permute-done.4.refs_6_), channel_id=1, source_target_pairs={{0,1},{1,2},{2,3},{3,4},{4,5},{5,6},{6,7},{7,0},{8,9},{9,10},{10,1... | collective-permute-start | bytes 196616 | tf_op jit(solution)/shard_map/ppermute | solution.py:100
  35.6 4.3 %collective-permute-start.2 = (bf16[128,256]{1,0:T(8,128)(2,1)S(1)}, bf16[128,256]{1,0:T(8,128)(2,1)S(1)}, u32[]{:S(2)}, u32[]{:S(2)}) collective-permute-start(bf16[128,256]{1,0:T(8,128)(2,1)S(1)} %collective-permute-done.1.refs_2_), channel_id=1, source_target_pairs={{0,7},{1,0},{2,1},{3,2},{4,3},{5,4},{6,5},{7,6},{8,15},{9,8},{10,9... | collective-permute-start | bytes 196616 | tf_op jit(solution)/shard_map/ppermute | solution.py:102
  38.3 0.7 copy-start.2
  41.0 14.1 %all-to-all-start.1 = ((f16[8,160,128]{2,1,0:T(8,128)(2,1)}), f16[8,160,128]{2,1,0:T(8,128)(2,1)S(1)}, u32[]{:S(2)}, u32[]{:S(2)}) async-start(f16[8,160,128]{2,1,0:T(8,128)(2,1)} %convert_element_type.21), calls=%async_computation.1 | async-start | bytes 655360 | tf_op jit(solution)/shard_map/all_to_all | solution.py:29
  47.3 57.2 %copy-start = (bf16[272,512]{1,0:T(8,128)(2,1)S(1)}, bf16[272,512]{1,0:T(8,128)(2,1)}, u32[]{:S(2)}) copy-start(bf16[272,512]{1,0:T(8,128)(2,1)} %pack.1.refs_0_) | copy-start | bytes 835588
  47.4 16.7 %collective-permute-start.10 = (bf16[272,512]{1,0:T(8,128)(2,1)}, bf16[272,512]{1,0:T(8,128)(2,1)S(1)}, u32[]{:S(2)}, u32[]{:S(2)}) collective-permute-start(bf16[272,512]{1,0:T(8,128)(2,1)} %pack.1.refs_0_), channel_id=1, source_target_pairs={{0,1},{1,2},{2,3},{3,4},{4,5},{5,6},{6,7},{7,0},{8,9},{9,10},{10,1... | collective-permute-start | bytes 835592 | tf_op jit(solution)/shard_map/ppermute | solution.py:100
  48.9 11.0 %collective-permute-start.6 = (bf16[128,256]{1,0:T(8,128)(2,1)S(1)}, bf16[128,256]{1,0:T(8,128)(2,1)S(1)}, u32[]{:S(2)}, u32[]{:S(2)}) collective-permute-start(bf16[128,256]{1,0:T(8,128)(2,1)S(1)} %collective-permute-done.5.refs_5_), channel_id=1, source_target_pairs={{0,1},{1,2},{2,3},{3,4},{4,5},{5,6},{6,7},{7,0},{8,9},{9,10},{10,1... | collective-permute-start | bytes 196616 | tf_op jit(solution)/shard_map/ppermute | solution.py:100
  50.2 14.5 %collective-permute-start.7 = (bf16[272,512]{1,0:T(8,128)(2,1)}, bf16[272,512]{1,0:T(8,128)(2,1)S(1)}, u32[]{:S(2)}, u32[]{:S(2)}) collective-permute-start(bf16[272,512]{1,0:T(8,128)(2,1)} %pack.1.refs_0_), channel_id=1, source_target_pairs={{0,7},{1,0},{2,1},{3,2},{4,3},{5,4},{6,5},{7,6},{8,15},{9,8},{10,9... | collective-permute-start | bytes 835592 | tf_op jit(solution)/shard_map/ppermute | solution.py:102
  64.1 6.7 %collective-permute-start.11 = (bf16[272,512]{1,0:T(8,128)(2,1)S(1)}, bf16[272,512]{1,0:T(8,128)(2,1)S(1)}, u32[]{:S(2)}, u32[]{:S(2)}) collective-permute-start(bf16[272,512]{1,0:T(8,128)(2,1)S(1)} %collective-permute-done.10.refs_7_), channel_id=1, source_target_pairs={{0,1},{1,2},{2,3},{3,4},{4,5},{5,6},{6,7},{7,0},{8,9},{9,10},{10,1... | collective-permute-start | bytes 835592 | tf_op jit(solution)/shard_map/ppermute | solution.py:100
  64.7 19.2 %collective-permute-start.8 = (bf16[272,512]{1,0:T(8,128)(2,1)S(1)}, bf16[272,512]{1,0:T(8,128)(2,1)S(1)}, u32[]{:S(2)}, u32[]{:S(2)}) collective-permute-start(bf16[272,512]{1,0:T(8,128)(2,1)S(1)} %collective-permute-done.7.refs_1_), channel_id=1, source_target_pairs={{0,7},{1,0},{2,1},{3,2},{4,3},{5,4},{6,5},{7,6},{8,15},{9,8},{10,9... | collective-permute-start | bytes 835592 | tf_op jit(solution)/shard_map/ppermute | solution.py:102
  70.8 16.3 %collective-permute-start.12 = (bf16[272,512]{1,0:T(8,128)(2,1)S(1)}, bf16[272,512]{1,0:T(8,128)(2,1)S(1)}, u32[]{:S(2)}, u32[]{:S(2)}) collective-permute-start(bf16[272,512]{1,0:T(8,128)(2,1)S(1)} %collective-permute-done.11.refs_6_), channel_id=1, source_target_pairs={{0,1},{1,2},{2,3},{3,4},{4,5},{5,6},{6,7},{7,0},{8,9},{9,10},{10,1... | collective-permute-start | bytes 835592 | tf_op jit(solution)/shard_map/ppermute | solution.py:100
  71.5 21.4 %all-to-all-start.2 = ((f16[16,32,128]{2,1,0:T(8,128)(2,1)}), f16[16,32,128]{2,1,0:T(8,128)(2,1)S(1)}, u32[]{:S(2)}, u32[]{:S(2)}) async-start(f16[16,32,128]{2,1,0:T(8,128)(2,1)} %convert_element_type.24), calls=%async_computation.2 | async-start | bytes 262144 | tf_op jit(solution)/shard_map/all_to_all | solution.py:29
  84.0 20.5 %collective-permute-start.9 = (bf16[272,512]{1,0:T(8,128)(2,1)S(1)}, bf16[272,512]{1,0:T(8,128)(2,1)S(1)}, u32[]{:S(2)}, u32[]{:S(2)}) collective-permute-start(bf16[272,512]{1,0:T(8,128)(2,1)S(1)} %collective-permute-done.8.refs_2_), channel_id=1, source_target_pairs={{0,7},{1,0},{2,1},{3,2},{4,3},{5,4},{6,5},{7,6},{8,15},{9,8},{10,9... | collective-permute-start | bytes 835592 | tf_op jit(solution)/shard_map/ppermute | solution.py:102
  87.0 17.5 %collective-permute-start.13 = (bf16[272,512]{1,0:T(8,128)(2,1)S(1)}, bf16[272,512]{1,0:T(8,128)(2,1)S(1)}, u32[]{:S(2)}, u32[]{:S(2)}) collective-permute-start(bf16[272,512]{1,0:T(8,128)(2,1)S(1)} %collective-permute-done.12.refs_5_), channel_id=1, source_target_pairs={{0,1},{1,2},{2,3},{3,4},{4,5},{5,6},{6,7},{7,0},{8,9},{9,10},{10,1... | collective-permute-start | bytes 835592 | tf_op jit(solution)/shard_map/ppermute | solution.py:100
  104.5 18.5 %copy-start.1 = (bf16[2,128,256]{2,1,0:T(8,128)(2,1)S(1)}, bf16[2,128,256]{2,1,0:T(8,128)(2,1)}, u32[]{:S(2)}) copy-start(bf16[2,128,256]{2,1,0:T(8,128)(2,1)} %w_ref.1) | copy-start | bytes 393220
